TPU v7x, 32 devices: a whole 2x2x4 slice. The times are simulated.
32 devices in a mesh: grp: 2 (over y), sp: 4 (over z), tp: 4 (over x, core).
Axes of the slice: x: 2, y: 2, z: 4, core: 2. Of those that a mesh axis runs over, the one named last changes fastest.
Arguments:
- latent: bfloat16 [4096, 2048], P(('grp', 'sp', 'tp')), parts along dimension 0, may hold values from -3 to 3
- context: bfloat16 [1024, 2048], P(('grp', 'sp')), parts along dimension 0, may hold values from -6 to 6
- condition: float32 [4096], P(('grp', 'sp')), parts along dimension 0, may hold values from -6 to 6
- context_condition: float32 [2048], P('sp'), may hold values from -6 to 6
- mod_weight: bfloat16 [2048, 6144], P('sp', 'tp'), may hold values from -0.1875 to 0.1875
- mod_bias: float32 [6144], replicated, may hold values from -1.5 to 1.5
- query_weight: bfloat16 [2048, 1024], P('sp'), may hold values from -0.125 to 0.125
- key_weight: bfloat16 [2048, 1024], P('sp'), may hold values from -0.125 to 0.125
- value_weight: bfloat16 [2048, 2048], P(None, 'tp'), may hold values from -3 to 3
- out_gate_weight: bfloat16 [2048, 2048], P(None, 'tp'), may hold values from -0.125 to 0.125
- decay_in_weight: bfloat16 [2048, 32], replicated, may hold values from -0.125 to 0.125
- decay_weight: bfloat16 [2, 16, 1024], replicated, may hold values from -1.5 to 1.5
- decay_bias: float32 [2, 1024], replicated, may hold values from 0.5 to 11
- extra_decay: float32 [2, 4, 2048], P(None, None, 'sp'), may hold values from -2.1 to 0
- norm_gain: float32 [512], replicated, may hold values from 0.1 to 1.9
- out_weight: bfloat16 [2048, 2048], P('tp'), may hold values from -0.25 to 0.25
- final_gain: float32 [2048], replicated, may hold values from 0.1 to 1.9
- final_bias: float32 [2048], replicated, may hold values from -1.5 to 1.5
Outputs:
- output: bfloat16 [4096, 2048], P(('grp', 'sp', 'tp')), parts along dimension 0
There are 2 independent parts, one for each index of `grp`. A program takes and returns all parts, laid end to end along the dimension named above; an argument that names none is the same for every part. Nothing has to cross between parts.
All inputs are finite; a program needn't handle non-finite values.
Results may differ from a plain program's by a relative error of at most 0.012.
The roundings to bfloat16 on the way count: a program that leaves them out, or rounds other values in their place, can miss the bound.
Values may be sent and summed in bfloat16 or wider, within the bound.
A program may use at most 64 MiB of HBM per device.

v0:
```python
import jax
import jax.numpy as jnp
from jax import lax
from jax.sharding import PartitionSpec as P

ATTENTION_HEADS = 4
DV = 512
BLOCK = 64
GRID_W = 64


norm_eps = 1e-05
gate_scale = 16.0
rope_base = 10000.0
residual_scale = 2.0**0.5
highest = lax.Precision.HIGHEST


def entering(part, axis, combine, identity, reverse):
    count = lax.axis_size(axis)
    place = lax.axis_index(axis)
    ahead = count - 1 - place if reverse else place
    gathered = jax.tree.map(lambda a: lax.all_gather(a, axis), part)
    state = jax.tree.map(lambda a, e: jnp.zeros_like(a) + jnp.asarray(e, a.dtype), part, identity)

    def one(lap, state):
        source = count - 1 - lap if reverse else lap
        return combine(
            state, jax.tree.map(lambda a: lax.dynamic_index_in_dim(a, source, 0, False), gathered)
        )

    return lax.fori_loop(0, ahead, one, state)


def rotate_half(values, angle):
    half_width = values.shape[-1] // 2
    first_half = values[..., :half_width]
    second_half = values[..., half_width:]
    cosine = jnp.cos(angle)
    sine_part = jnp.sin(angle)
    return jnp.concatenate(
        [
            first_half * cosine - second_half * sine_part,
            first_half * sine_part + second_half * cosine,
        ],
        axis=-1,
    )


def rotary(values, token_places):
    quarter = values.shape[-1] // 4
    frequency = rope_base ** (-jnp.arange(quarter, dtype=jnp.float32) / quarter)
    row_index = (token_places // GRID_W).astype(jnp.float32)
    col_index = (token_places % GRID_W).astype(jnp.float32)
    half_width = 2 * quarter
    by_row = rotate_half(values[..., :half_width], row_index[:, None] * frequency)
    by_col = rotate_half(values[..., half_width:], col_index[:, None] * frequency)
    return jnp.concatenate([by_row, by_col], axis=-1)


def log_decays(low_rank, decay_weight, decay_bias):
    rank_width = decay_weight.shape[1]
    decay_parts = []
    for direction in range(2):
        logits = (
            jnp.dot(
                low_rank[:, direction * rank_width : (direction + 1) * rank_width],
                decay_weight[direction],
                preferred_element_type=jnp.float32,
            )
            + decay_bias[direction]
        )
        decay_parts.append(jax.nn.log_sigmoid(logits) / gate_scale)
    return decay_parts


def flip_rows(values):
    return jnp.flip(values, axis=0)


def end_state(key_rows, value_rows, logdec):
    cumulative = jnp.cumsum(logdec, axis=0)
    total_decay = cumulative[-1]
    weights = jnp.exp(total_decay - cumulative)
    return (total_decay, jnp.einsum("nd,nv->dv", key_rows * weights, value_rows, precision=highest))


def join_states(earlier, later):
    return (earlier[0] + later[0], jnp.exp(later[0])[:, None] * earlier[1] + later[1])


def blocked_scan(queries, key_rows, value_rows, logdec, start):
    block_count = queries.shape[0] // BLOCK
    lower_mask = jnp.tril(jnp.ones((BLOCK, BLOCK), dtype=bool))

    def blocks(values):
        return values.reshape(block_count, BLOCK, values.shape[1])

    def advance(carry_state, block_data):
        query_block, key_block, value_block, decay_block = block_data
        cumulative = jnp.cumsum(decay_block, axis=0)
        total_decay = cumulative[-1]
        query_decayed = query_block * jnp.exp(cumulative)
        key_inverse = key_block * jnp.exp(-cumulative)
        key_closing = key_block * jnp.exp(total_decay - cumulative)
        scores = jnp.einsum("cd,sd->cs", query_decayed, key_inverse, precision=highest)
        scores = jnp.where(lower_mask, scores, 0.0)
        outputs = jnp.einsum("cs,sv->cv", scores, value_block, precision=highest) + jnp.einsum(
            "cd,dv->cv", query_decayed, carry_state, precision=highest
        )
        carry_state = jnp.exp(total_decay)[:, None] * carry_state + jnp.einsum(
            "cd,cv->dv", key_closing, value_block, precision=highest
        )
        return (carry_state, outputs)

    unused_state, outputs = lax.scan(
        advance, start, (blocks(queries), blocks(key_rows), blocks(value_rows), blocks(logdec))
    )
    return outputs.reshape(queries.shape[0], value_rows.shape[1])


def body(
    latent,
    context,
    condition,
    context_condition,
    mod_weight,
    mod_bias,
    query_weight,
    key_weight,
    value_weight,
    out_gate_weight,
    decay_in_weight,
    decay_weight,
    decay_bias,
    extra_decay,
    norm_gain,
    out_weight,
    final_gain,
    final_bias,
):
    model_width = latent.shape[1]
    head_keys = query_weight.shape[1] // ATTENTION_HEADS
    value_cols = value_weight.shape[1]
    tp_index = lax.axis_index("tp")
    head_share = lax.axis_size("tp") // ATTENTION_HEADS
    head_index = tp_index // head_share
    part_index = tp_index % head_share
    activated = jax.nn.silu(jnp.stack([condition, context_condition])).astype(jnp.bfloat16)
    partial_value = jnp.dot(activated, mod_weight, preferred_element_type=jnp.float32)
    row_sums = lax.psum(partial_value, "sp")
    modulation = lax.all_gather(row_sums, "tp", axis=1, tiled=True)
    modulation = modulation + mod_bias
    shifts = modulation[:, :model_width]
    scales = modulation[:, model_width : 2 * model_width]
    branch_gate = modulation[0, 2 * model_width :]
    mod_latent = (latent.astype(jnp.float32) * (1.0 + scales[0]) + shifts[0]).astype(jnp.bfloat16)
    mod_context = (context.astype(jnp.float32) * (1.0 + scales[1]) + shifts[1]).astype(jnp.bfloat16)
    key_start = head_index * head_keys
    query_slice = lax.dynamic_slice_in_dim(query_weight, key_start, head_keys, 1)
    key_slice = lax.dynamic_slice_in_dim(key_weight, key_start, head_keys, 1)
    query_head, key_head = (
        lax.all_gather(query_slice, "sp", axis=0, tiled=True),
        lax.all_gather(key_slice, "sp", axis=0, tiled=True),
    )
    combined = jnp.concatenate(
        [query_head, out_gate_weight, key_head, value_weight, decay_in_weight], axis=1
    )
    offset = head_keys + value_cols
    projected = jnp.dot(
        lax.all_gather(mod_latent, "tp", axis=0, tiled=True),
        combined,
        preferred_element_type=jnp.float32,
    ).astype(jnp.bfloat16)
    context_local = jnp.dot(
        mod_context, combined[:, offset:], preferred_element_type=jnp.float32
    ).astype(jnp.bfloat16)
    gathered_context = lax.all_gather(context_local, "sp", axis=0, tiled=True)
    queries = projected[:, :head_keys].astype(jnp.float32) * head_keys ** (-0.5)
    out_gate = projected[:, head_keys:offset]
    key_rows = projected[:, offset : offset + head_keys].astype(jnp.float32)
    value_rows = projected[:, offset + head_keys : offset + head_keys + value_cols].astype(
        jnp.float32
    )
    low_rank = projected[:, offset + head_keys + value_cols :]
    token_places = lax.axis_index("sp") * projected.shape[0] + jnp.arange(
        projected.shape[0], dtype=jnp.int32
    )
    queries = rotary(queries, token_places)
    key_rows = rotary(key_rows, token_places)
    head_bias = lax.dynamic_slice_in_dim(decay_bias, key_start, head_keys, 1)
    head_gate = lax.dynamic_slice_in_dim(decay_weight, key_start, head_keys, 2)
    head_extra = lax.dynamic_index_in_dim(extra_decay, head_index, 1, keepdims=False)
    latent_decay = log_decays(low_rank, head_gate, head_bias)
    forward_decay = latent_decay[0] + head_extra[0][:, None]
    backward_decay = latent_decay[1] + head_extra[1][:, None]
    context_keys = gathered_context[:, :head_keys].astype(jnp.float32)
    context_values = gathered_context[:, head_keys : head_keys + value_cols].astype(jnp.float32)
    context_decay = log_decays(gathered_context[:, head_keys + value_cols :], head_gate, head_bias)
    context_forward = end_state(context_keys, context_values, context_decay[0])[1]
    context_backward = end_state(
        flip_rows(context_keys), flip_rows(context_values), flip_rows(context_decay[1])
    )[1]
    forward_total, forward_state = end_state(key_rows, value_rows, forward_decay)
    backward_total, backward_state = end_state(
        flip_rows(key_rows), flip_rows(value_rows), flip_rows(backward_decay)
    )
    identity = (
        jnp.zeros((head_keys,), jnp.float32),
        jnp.zeros((head_keys, value_cols), jnp.float32),
    )
    arrived_forward = entering((forward_total, forward_state), "sp", join_states, identity, False)
    arrived_backward = entering((backward_total, backward_state), "sp", join_states, identity, True)
    start_forward = jnp.exp(arrived_forward[0])[:, None] * context_forward + arrived_forward[1]
    start_backward = jnp.exp(arrived_backward[0])[:, None] * context_backward + arrived_backward[1]
    out_forward = blocked_scan(queries, key_rows, value_rows, forward_decay, start_forward)
    out_backward = flip_rows(
        blocked_scan(
            flip_rows(queries),
            flip_rows(key_rows),
            flip_rows(value_rows),
            flip_rows(backward_decay),
            start_backward,
        )
    )
    mixture = out_forward + out_backward
    squares = jnp.sum(mixture * mixture, axis=1)
    onehot = (jnp.arange(ATTENTION_HEADS) == head_index).astype(jnp.float32)
    totals = lax.psum(onehot[:, None] * squares[None, :], "tp")
    head_sum = jnp.sum(totals * onehot[:, None], axis=0)
    gain_slice = lax.dynamic_slice_in_dim(norm_gain, part_index * value_cols, value_cols, 0)
    normed = mixture * lax.rsqrt(head_sum / DV + norm_eps)[:, None] * gain_slice
    gated_rows = (normed * jax.nn.silu(out_gate.astype(jnp.float32))).astype(jnp.bfloat16)
    regrouped = lax.all_to_all(gated_rows, "tp", split_axis=0, concat_axis=1, tiled=True)
    branch = jnp.dot(
        regrouped,
        lax.all_gather(out_weight, "tp", axis=0, tiled=True),
        preferred_element_type=jnp.float32,
    )
    summed = residual_scale * latent.astype(jnp.float32) + branch_gate * branch
    row_mean = jnp.mean(summed, axis=1, keepdims=True)
    centered = summed - row_mean
    variance = jnp.mean(centered * centered, axis=1, keepdims=True)
    return (centered * lax.rsqrt(variance + norm_eps) * final_gain + final_bias).astype(
        jnp.bfloat16
    )


def solution(mesh):
    placed = (
        P(("grp", "sp", "tp"), None),
        P(("grp", "sp"), None),
        P(("grp", "sp")),
        P("sp"),
        P("sp", "tp"),
        P(),
        P("sp", None),
        P("sp", None),
        P(None, "tp"),
        P(None, "tp"),
        P(),
        P(),
        P(),
        P(None, None, "sp"),
        P(),
        P("tp", None),
        P(),
        P(),
    )
    return jax.shard_map(
        body, mesh=mesh, in_specs=placed, out_specs=P(("grp", "sp", "tp"), None), check_vma=False
    )
```

profile of v0, /device:TPU:0, one launch (start us, length us, event | category | flops | bytes accessed | tf_op | source)
XLA Modules:
  0.0 400.8 jit_solution(14803225204170053554)
XLA Ops:
  6.6 1.8 constant_dynamic-slice_fusion.6
  8.5 1.7 constant_dynamic-slice_fusion.5
  11.3 21.0 %psum.14 = f32[2,1536]{1,0:T(2,128)S(1)} all-reduce(f32[2,1536]{1,0:T(2,128)S(1)} %fusion.151), channel_id=1, replica_groups=mesh['grp'=2,'sp'=4,'tp'=4] {'sp'}, use_global_device_ids=true, to_apply=%region_0.1 | all-reduce | flops 3072 | bytes 24576 | tf_op jit(solution)/shard_map/psum | solution.py:151
  32.2 5.2 %all_gather.36 = f32[2,6144]{1,0:T(2,128)S(1)} all-gather(f32[2,1536]{1,0:T(2,128)S(1)} %psum.14), channel_id=1, replica_groups=mesh['grp'=2,'sp'=4,'tp'=4] {'tp'}, dimensions={1}, use_global_device_ids=true | all-gather | bytes 61440 | tf_op jit(solution)/shard_map/all_gather | solution.py:152
  40.0 1.3 fusion.169
  43.2 2.5 constant_dynamic-update-slice_fusion.4
  45.7 1.5 constant_dynamic-update-slice_fusion.3
  47.2 21.7 %all-gather.15.cloned.1.call-done = bf16[2048,256]{1,0:T(8,128)(2,1)} async-done(((bf16[512,256]{1,0:T(8,128)(2,1)}), bf16[2048,256]{1,0:T(8,128)(2,1)}) %all-gather.15.cloned.1.call-update) | async-done | bytes 1048592 | tf_op jit(solution)/shard_map/all_gather | solution.py:164
  68.9 2.3 constant_dynamic-update-slice_fusion.2
  71.2 3.1 constant_dynamic-update-slice_fusion.1
  75.2 17.2 %all-gather.11.cloned.1.call-done = bf16[512,2048]{1,0:T(8,128)(2,1)} async-done(((bf16[128,2048]{1,0:T(8,128)(2,1)}), bf16[512,2048]{1,0:T(8,128)(2,1)}) %all-gather.11.cloned.1.call-update) | async-done | bytes 2097168 | tf_op jit(solution)/shard_map/all_gather | solution.py:171
  92.4 7.1 %convolution_convert_fusion = bf16[512,1568]{0,1:T(8,128)(2,1)S(1)} fusion(bf16[512,2048]{1,0:T(8,128)(2,1)} %all-gather.11.cloned.1.call-done, bf16[2048,1568]{1,0:T(8,128)(2,1)} %constant_dynamic-update-slice_fusion), kind=kOutput, calls=%fused_computation.80 | convolution fusion | flops 3289137152 | bytes 10125312 | tf_op jit(solution)/shard_map/dot_general | solution.py:170
  105.9 2.8 fusion.138
  111.0 1.5 rev.31
  112.5 1.9 fusion.102
  114.5 2.2 fusion.85
  122.3 2.1 copy.93
  126.2 2.7 fusion.111
  129.5 3.6 fusion.73
  133.1 39.0 %all_gather.43 = bf16[512,800]{0,1:T(8,128)(2,1)S(1)} all-gather(bf16[128,800]{0,1:T(8,128)(2,1)S(1)} %fusion.73), channel_id=1, replica_groups=mesh['grp'=2,'sp'=4,'tp'=4] {'sp'}, dimensions={0}, use_global_device_ids=true | all-gather | bytes 1024000 | tf_op jit(solution)/shard_map/all_gather | solution.py:178
  172.1 2.0 fusion.94
  176.1 2.0 fusion.87
  178.1 5.1 %reverse.3 = f32[512,256]{0,1:T(8,128)} reverse(f32[512,256]{0,1:T(8,128)} %fusion.94), dimensions={0} | reverse | bytes 1048576 | tf_op jit(solution)/shard_map/reverse
  183.2 1.9 multiply_bitcast_fusion
  185.1 2.0 reshape.290
  187.1 2.0 copy.105
  191.2 1.9 broadcast_add_fusion
  193.1 2.0 copy.106
  196.4 9.4 %rev.34 = f32[512,512]{0,1:T(8,128)} reverse(f32[512,512]{0,1:T(8,128)} %slice_convert_fusion), dimensions={0} | reverse | bytes 2097152 | tf_op jit(solution)/shard_map/jit(_flip)/rev | solution.py:78
  205.7 5.0 %rev.32 = f32[512,256]{0,1:T(8,128)} reverse(f32[512,256]{0,1:T(8,128)} %slice_convert_fusion.2), dimensions={0} | reverse | bytes 1048576 | tf_op jit(solution)/shard_map/jit(_flip)/rev | solution.py:78
  210.8 2.0 reshape.281
  212.8 2.0 copy.95
  216.8 1.9 broadcast_add_fusion.2
  218.7 2.0 copy.96
  223.0 2.1 copy.107
  231.8 9.7 %all-gather.3 = f32[4,1,256]{2,1,0:T(1,128)S(1)} all-gather(f32[1,1,256]{2,1,0:T(1,128)S(1)} %bitcast.368), channel_id=1, replica_groups=mesh['grp'=2,'sp'=4,'tp'=4] {'sp'}, dimensions={0}, use_global_device_ids=true | all-gather | bytes 5120 | tf_op jit(solution)/shard_map/all_gather | solution.py:23
  242.5 7.6 %all-gather.2 = f32[4,1,256]{2,1,0:T(1,128)S(1)} all-gather(f32[1,1,256]{2,1,0:T(1,128)S(1)} %bitcast.373), channel_id=1, replica_groups=mesh['grp'=2,'sp'=4,'tp'=4] {'sp'}, dimensions={0}, use_global_device_ids=true | all-gather | bytes 5120 | tf_op jit(solution)/shard_map/all_gather | solution.py:23
  251.5 3.9 while.53
  255.4 2.2 fusion.67
  257.7 49.8 %while.55 = (s32[]{:T(128)}, f32[256,512]{1,0:T(8,128)S(1)}, f32[8,64,512]{2,1,0:T(8,128)S(1)}, f32[8,64,256]{2,1,0:T(8,128)}, f32[8,64,256]{2,1,0:T(8,128)}, /*...) while((s32[]{:T(128)}, f32[256,512]{1,0:T(8,128)S(1)}, ...), condition=%wide.region_18.19_spmd.clone, body=%wide.region_16.18_spmd.clone.sunk | while | flops 240508928 | bytes 3057253 | solution.py:116
  262.3 1.7 convolution_add_fusion.11
  268.5 1.7 convolution_add_fusion.11
  274.7 1.7 convolution_add_fusion.11
  280.9 1.7 convolution_add_fusion.11
  287.2 1.7 convolution_add_fusion.11
  293.4 1.7 convolution_add_fusion.11
  299.6 1.7 convolution_add_fusion.11
  305.8 1.7 convolution_add_fusion.11
  307.9 5.9 %rev.36 = f32[512,512]{0,1:T(8,128)} reverse(f32[512,512]{0,1:T(8,128)S(1)} %copy.111), dimensions={0} | reverse | bytes 2097152 | tf_op jit(solution)/shard_map/jit(_flip)/rev | solution.py:78
  315.7 49.8 %while.54 = (s32[]{:T(128)}, f32[256,512]{1,0:T(8,128)S(1)}, f32[8,64,512]{2,1,0:T(8,128)S(1)}, f32[8,64,256]{2,1,0:T(8,128)}, f32[8,64,256]{2,1,0:T(8,128)}, /*...) while((s32[]{:T(128)}, f32[256,512]{1,0:T(8,128)S(1)}, ...), condition=%wide.region_9.10_spmd.clone, body=%wide.region_7.9_spmd.clone.sunk | while | flops 240508928 | bytes 3057253 | solution.py:116
  320.2 1.7 convolution_add_fusion.10
  326.4 1.7 convolution_add_fusion.10
  332.7 1.7 convolution_add_fusion.10
  338.9 1.7 convolution_add_fusion.10
  345.1 1.7 convolution_add_fusion.10
  351.3 1.7 convolution_add_fusion.10
  357.6 1.7 convolution_add_fusion.10
  363.8 1.7 convolution_add_fusion.10
  365.5 1.3 copy.112
  366.8 1.9 multiply_reduce_fusion.1
  368.8 5.7 %psum.15 = f32[4,512]{1,0:T(4,128)S(1)} all-reduce(f32[4,512]{1,0:T(4,128)S(1)} %broadcast_multiply_fusion), channel_id=1, replica_groups=mesh['grp'=2,'sp'=4,'tp'=4] {'tp'}, use_global_device_ids=true, to_apply=%region_20.21 | all-reduce | flops 2048 | bytes 16384 | tf_op jit(solution)/shard_map/psum | solution.py:229
  374.6 1.4 copy_bitcast_fusion
  376.0 11.6 %all_to_all.19 = bf16[4,128,512]{1,2,0:T(8,128)(2,1)S(1)} all-to-all(bf16[4,128,512]{1,2,0:T(8,128)(2,1)S(1)} %copy_bitcast_fusion), channel_id=1, replica_groups=mesh['grp'=2,'sp'=4,'tp'=4] {'tp'}, dimensions={0} | all-to-all | bytes 1048576 | tf_op jit(solution)/shard_map/all_to_all | solution.py:234
  387.7 4.9 %fusion.170 = (f32[128]{0:T(128)S(1)}, f32[128,2048]{1,0:T(8,128)S(1)}) fusion(bf16[128,2048]{0,1:T(8,128)(2,1)S(1)} %bitcast.330, bf16[2048,2048]{1,0:T(8,128)(2,1)} %all-gather.17.cloned.1.call-done, f32[2048]{0:T(1024)S(1)} %bitcast.359, bf16[128,2048]{1,0:T(8,128)(2,1)S(1)} %copy-done.11), kind=kOutput, calls=%fused_computation.266 | convolution fusion | flops 1075052416 | bytes 10494464 | tf_op jit(solution)/shard_map/dot_general | solution.py:235
  (287 shorter events, 121.2 us)
Async XLA Ops:
  6.5 3.7 copy-start
  6.5 30.9 %copy-start.19 = (f32[6144]{0:T(1024)S(1)}, f32[6144]{0:T(1024)}, u32[]{:S(2)}) copy-start(f32[6144]{0:T(1024)} %param.31) | copy-start | bytes 73732
  6.5 31.6 %copy-start.10 = (bf16[128,2048]{1,0:T(8,128)(2,1)S(1)}, bf16[128,2048]{1,0:T(8,128)(2,1)}, u32[]{:S(2)}) copy-start(bf16[128,2048]{1,0:T(8,128)(2,1)} %param.26) | copy-start | bytes 1572868
  6.5 32.6 %copy-start.18 = (bf16[2048,32]{0,1:T(8,128)(2,1)S(1)}, bf16[2048,32]{0,1:T(8,128)(2,1)}, u32[]{:S(2)}) copy-start(bf16[2048,32]{0,1:T(8,128)(2,1)} %param.36) | copy-start | bytes 393220
  6.5 36.7 %all-gather.13.cloned.1.call-start = ((), (), s32[]{:S(2)}) async-start(), calls=%async_computation.2 | async-start | bytes 1310720 | tf_op jit(solution)/shard_map/all_gather | solution.py:163
  8.4 60.4 %all-gather.15.cloned.1.call-start = ((), (), s32[]{:S(2)}) async-start(), calls=%async_computation.3 | async-start | bytes 1310720 | tf_op jit(solution)/shard_map/all_gather | solution.py:164
  10.2 82.2 %all-gather.11.cloned.1.call-start = ((), (), s32[]{:S(2)}) async-start(), calls=%async_computation.1 | async-start | bytes 2621440 | tf_op jit(solution)/shard_map/all_gather | solution.py:171
  39.1 212.3 %all-gather.21.cloned.1.call-start = ((), (), s32[]{:S(2)}) async-start(), calls=%async_computation.6 | async-start | bytes 2621440 | tf_op jit(solution)/shard_map/all_gather | solution.py:23
  39.4 34.9 %copy-start.12 = (bf16[2048,32]{1,0:T(8,128)(2,1)}, bf16[2048,32]{1,0:T(8,128)(2,1)S(1)}, u32[]{:S(2)}) copy-start(bf16[2048,32]{1,0:T(8,128)(2,1)S(1)} %copy.90) | copy-start | bytes 393220
  41.4 59.4 %copy-start.31 = (f32[1,256]{1,0:T(1,128)}, f32[1,256]{1,0:T(1,128)S(1)}, u32[]{:S(2)}) copy-start(f32[1,256]{1,0:T(1,128)S(1)} %get-tuple-element.333) | copy-start | bytes 3076
  43.2 2.5 copy-start.14
  99.5 1.3 copy-start.15
  102.9 6.5 %copy-start.2 = (f32[512,256]{0,1:T(8,128)}, f32[512,256]{0,1:T(8,128)S(1)}, u32[]{:S(2)}) copy-start(f32[512,256]{0,1:T(8,128)S(1)} %rev.29) | copy-start | bytes 1572868
  105.9 8.6 %copy-start.20 = (f32[256]{0:T(256)}, f32[256]{0:T(256)S(1)}, u32[]{:S(2)}) copy-start(f32[256]{0:T(256)S(1)} %slice_reduce_fusion.1) | copy-start | bytes 3076
  108.7 0.7 copy-start.17
  109.4 0.8 copy-start.3
  110.2 4.3 %copy-start.24 = (f32[1,1,512]{2,1,0:T(1,128)S(1)}, f32[1,1,512]{2,1,0:T(1,128)}, u32[]{:S(2)}) copy-start(f32[1,1,512]{2,1,0:T(1,128)} %get-tuple-element.332) | copy-start | bytes 6148
  114.4 199.4 %all-gather.19.cloned.1.call-start = ((), (), s32[]{:S(2)}) async-start(), calls=%async_computation.5 | async-start | bytes 2621440 | tf_op jit(solution)/shard_map/all_gather | solution.py:23
  124.3 5.2 %copy-start.13 = (bf16[2048,32]{1,0:T(8,128)(2,1)S(1)}, bf16[2048,32]{1,0:T(8,128)(2,1)}, u32[]{:S(2)}) copy-start(bf16[2048,32]{1,0:T(8,128)(2,1)} %copy-done.12) | copy-start | bytes 393220
  124.3 5.2 %copy-start.26 = (f32[1,2048]{1,0:T(1,128)S(1)}, f32[1,2048]{1,0:T(1,128)}, u32[]{:S(2)}) copy-start(f32[1,2048]{1,0:T(1,128)} %get-tuple-element.327) | copy-start | bytes 24580
  125.7 0.5 copy-start.27
  128.9 258.8 %all-gather.17.cloned.1.call-start = ((), (), s32[]{:S(2)}) async-start(), calls=%async_computation.4 | async-start | bytes 10485760 | tf_op jit(solution)/shard_map/all_gather | solution.py:237
  129.5 42.6 %copy-start.32 = (f32[1,256]{1,0:T(1,128)S(1)}, f32[1,256]{1,0:T(1,128)}, u32[]{:S(2)}) copy-start(f32[1,256]{1,0:T(1,128)} %copy-done.31) | copy-start | bytes 3076
  133.1 43.0 %copy-start.30 = (f32[1,256]{1,0:T(1,128)S(1)}, f32[1,256]{1,0:T(1,128)}, u32[]{:S(2)}) copy-start(f32[1,256]{1,0:T(1,128)} %get-tuple-element.334) | copy-start | bytes 3076
  190.3 0.8 copy-start.8
  216.0 0.8 copy-start.9
  223.0 6.5 %copy-start.4 = (f32[512,256]{0,1:T(8,128)S(1)}, f32[512,256]{0,1:T(8,128)}, u32[]{:S(2)}) copy-start(f32[512,256]{0,1:T(8,128)} %copy-done.3) | copy-start | bytes 1572868
  226.4 5.4 %copy-start.21 = (f32[256]{0:T(256)S(1)}, f32[256]{0:T(256)}, u32[]{:S(2)}) copy-start(f32[256]{0:T(256)} %copy-done.20) | copy-start | bytes 3076
  227.7 14.8 %copy-start.28 = (f32[256]{0:T(256)S(1)}, f32[256]{0:T(256)}, u32[]{:S(2)}) copy-start(f32[256]{0:T(256)} %copy-done.27) | copy-start | bytes 3076
  227.7 22.4 %copy-start.25 = (f32[1,1,512]{2,1,0:T(1,128)S(1)}, f32[1,1,512]{2,1,0:T(1,128)}, u32[]{:S(2)}) copy-start(f32[1,1,512]{2,1,0:T(1,128)} %get-tuple-element.332) | copy-start | bytes 6148
  229.4 20.6 %copy-start.16 = (f32[512,256]{0,1:T(8,128)S(1)}, f32[512,256]{0,1:T(8,128)}, u32[]{:S(2)}) copy-start(f32[512,256]{0,1:T(8,128)} %get-tuple-element.340) | copy-start | bytes 1572868
  251.5 3.9 copy-start.6
  251.5 3.9 copy-start.7
  313.9 1.0 copy-start.5
  365.5 9.1 %copy-start.29 = (f32[512]{0:T(512)S(1)}, f32[512]{0:T(512)}, u32[]{:S(2)}) copy-start(f32[512]{0:T(512)} %param.40) | copy-start | bytes 6148
  366.8 20.9 %copy-start.11 = (bf16[128,2048]{1,0:T(8,128)(2,1)S(1)}, bf16[128,2048]{1,0:T(8,128)(2,1)}, u32[]{:S(2)}) copy-start(bf16[128,2048]{1,0:T(8,128)(2,1)} %param.26) | copy-start | bytes 1572868
  387.7 5.2 %copy-start.22 = (f32[2048]{0:T(1024)S(1)}, f32[2048]{0:T(1024)}, u32[]{:S(2)}) copy-start(f32[2048]{0:T(1024)} %param.43) | copy-start | bytes 24580
  387.7 5.2 %copy-start.23 = (f32[2048]{0:T(1024)S(1)}, f32[2048]{0:T(1024)}, u32[]{:S(2)}) copy-start(f32[2048]{0:T(1024)} %param.42) | copy-start | bytes 24580
  387.7 6.2 %copy-start.1 = (bf16[512,1536]{1,0:T(8,128)(2,1)S(1)}, bf16[512,1536]{1,0:T(8,128)(2,1)}, u32[]{:S(2)}) copy-start(bf16[512,1536]{1,0:T(8,128)(2,1)} %param.30) | copy-start | bytes 4718596
Sparse Core Ops, SparseCore 0:
  8.9 31.1 all-gather.12
  41.6 27.1 all-gather.14
  70.4 21.9 all-gather.10
  114.5 58.8 all-gather.20
  174.8 44.4 all-gather.18
  220.7 57.0 all-gather.16
where the time goes:
time: 407 us; the launch traced here: 401 us
  matrix products  115 us (28%)
  blocking collectives  99.8 us (25%)
  local copies, waits for them, and re-layouts  98.8 us (24%)
  waiting for transfers between devices  39.3 us (10%)
  other arithmetic  32.2 us (8%)
  between operations  14 us (3%)
    all_gather x1, blocking collectives, body(): gathered_context = lax.all_gather(context_local, 'sp', axis=0, tiled=True)  39 us
    rev x11, local copies, waits for them, and re-layouts, flip_rows(): return jnp.flip(values, axis=0)  29.5 us
    dot_general x16, matrix products, advance(): jnp.einsum('cd,cv->dv', key_closing, value_block, precision=highest)  26.6 us
    another operation x21, local copies, waits for them, and re-layouts  21.9 us
    all_gather x1, waiting for transfers between devices, body(): lax.all_gather(key_slice, 'sp', axis=0, tiled=True)  21.7 us
    psum x1, blocking collectives, body(): row_sums = lax.psum(partial_value, 'sp')  21 us
    dot_general x16, matrix products, advance(): jnp.einsum('cd,dv->cv', query_decayed, carry_state, precision=highest)  20.7 us
    dot_general x16, matrix products, advance(): jnp.einsum('cs,sv->cv', scores, value_block, precision=highest)  18.7 us
  transfers between devices with their start and end apart: 6, of which 2 were waited for; matrix products, arithmetic and copies ran while one was open for 53% of the time, Pallas kernels for 0%

commit v1 on v0

v1 whole, which is shorter than its diff:
```python
import functools

import jax
import jax.numpy as jnp
from jax import lax
from jax.experimental import pallas as pl
from jax.experimental.pallas import tpu as pltpu
from jax.sharding import PartitionSpec as P

ATTENTION_HEADS = 4
DV = 512
BLOCK = 64
GRID_W = 64


norm_eps = 1e-05
gate_scale = 16.0
rope_base = 10000.0
residual_scale = 2.0**0.5
highest = lax.Precision.HIGHEST
f32 = jnp.float32
bf16 = jnp.bfloat16


def rope_tables(token_places, width):
    quarter = width // 4
    frequency = rope_base ** (-jnp.arange(quarter, dtype=f32) / quarter)
    row_angle = (token_places // GRID_W).astype(f32)[:, None] * frequency
    col_angle = (token_places % GRID_W).astype(f32)[:, None] * frequency
    cosine = jnp.concatenate([jnp.cos(row_angle)] * 2 + [jnp.cos(col_angle)] * 2, axis=1)
    row_sine, col_sine = jnp.sin(row_angle), jnp.sin(col_angle)
    sine = jnp.concatenate([-row_sine, row_sine, -col_sine, col_sine], axis=1)
    return cosine, sine


def dot(a, b, contract=((1,), (0,)), precision=None):
    return lax.dot_general(a, b, (contract, ((), ())), precision=precision,
                           preferred_element_type=f32)


def log_sigmoid(x):
    return jnp.minimum(x, 0.0) - jnp.log1p(jnp.exp(-jnp.abs(x)))


def rotate(x, cosine, sine):
    half = x.shape[1] // 2
    parts = [pltpu.roll(x[:, i * half:(i + 1) * half], half // 2, 1) for i in range(2)]
    return x * cosine + jnp.concatenate(parts, axis=1) * sine


def triangle(size, reverse):
    row = lax.broadcasted_iota(jnp.int32, (size, size), 0)
    col = lax.broadcasted_iota(jnp.int32, (size, size), 1)
    return row <= col if reverse else row >= col


def decay_block(low, decay_weight, decay_bias, direction):
    rank = decay_weight.shape[1]
    logits = dot(low[:, direction * rank:(direction + 1) * rank], decay_weight[direction])
    return log_sigmoid(logits + decay_bias[direction:direction + 1, :]) / gate_scale


def context_kernel(k_ref, v_ref, low_ref, dw_ref, db_ref, state_ref):
    length, width = k_ref.shape
    size = min(2 * BLOCK, length)
    count = length // size
    for direction in range(2):
        mask = triangle(size, direction == 1).astype(f32)
        edge = 0 if direction == 1 else size - 1
        state = None
        for step in range(count):
            b = count - 1 - step if direction == 1 else step
            rows = slice(b * size, (b + 1) * size)
            logdec = decay_block(low_ref[rows, :], dw_ref[...], db_ref[...], direction)
            cum = dot(mask, logdec, precision=highest)
            total = cum[edge:edge + 1, :]
            closing = (k_ref[rows, :].astype(f32) * jnp.exp(total - cum)).astype(bf16)
            term = dot(closing, v_ref[rows, :], ((0,), (0,)))
            state = term if state is None else jnp.exp(total).T * state + term
        state_ref[direction] = state


def local_kernel(q_ref, k_ref, v_ref, low_ref, extra_ref, dw_ref, db_ref, cos_ref, sin_ref,
                 out_ref, qc_ref, state_ref, total_ref):
    length, width = q_ref.shape
    size = 2 * BLOCK
    count = length // size
    rq, rk, within, scores = [], [], [], []
    for b in range(count):
        rows = slice(b * size, (b + 1) * size)
        cosine, sine = cos_ref[rows, :], sin_ref[rows, :]
        rq.append(rotate(q_ref[rows, :].astype(f32) * width ** -0.5, cosine, sine))
        rk.append(rotate(k_ref[rows, :].astype(f32), cosine, sine))
        scores.append(None)
    for direction in range(2):
        keep = triangle(size, direction == 1)
        mask = keep.astype(f32)
        edge = 0 if direction == 1 else size - 1
        middle = size // 2 if direction == 1 else size // 2 - 1
        state = None
        before = None
        for step in range(count):
            b = count - 1 - step if direction == 1 else step
            rows = slice(b * size, (b + 1) * size)
            logdec = decay_block(low_ref[rows, :], dw_ref[...], db_ref[...], direction)
            logdec = logdec + extra_ref[rows, direction:direction + 1]
            cum = dot(mask, logdec, precision=highest)
            total = cum[edge:edge + 1, :]
            center = cum[middle:middle + 1, :]
            q_mid = (rq[b] * jnp.exp(cum - center)).astype(bf16)
            k_mid = (rk[b] * jnp.exp(center - cum)).astype(bf16)
            score = jnp.where(keep, dot(q_mid, k_mid, ((1,), (1,))), 0.0)
            q_dec = rq[b] * jnp.exp(cum)
            if direction == 0:
                scores[b] = score
                out = None
            else:
                out = dot((scores[b] + score).astype(bf16), v_ref[rows, :])
            if state is not None:
                carried = dot(q_dec.astype(bf16), state.astype(bf16))
                out = carried if out is None else out + carried
            if direction == 0:
                out_ref[rows, :] = jnp.zeros((size, v_ref.shape[1]), f32) if out is None else out
            else:
                out_ref[rows, :] += out
            q_all = q_dec if before is None else q_dec * jnp.exp(before)
            qc_ref[rows, direction * width:(direction + 1) * width] = q_all.astype(bf16)
            closing = (rk[b] * jnp.exp(total - cum)).astype(bf16)
            term = dot(closing, v_ref[rows, :], ((0,), (0,)))
            state = term if state is None else jnp.exp(total).T * state + term
            before = total if before is None else before + total
        state_ref[direction * width:(direction + 1) * width, :] = state.astype(bf16)
        total_ref[direction:direction + 1, :] = before


def join_kernel(final, out_ref, qc_ref, states_ref, totals_ref, start_ref, gate_ref, gain_ref,
                place_ref, result_ref):
    count = states_ref.shape[0]
    width = qc_ref.shape[1] // 2
    place = place_ref[...]
    mixture = out_ref[...]
    for direction in range(2):
        state = start_ref[direction]
        for lap in range(count):
            j = count - 1 - lap if direction == 1 else lap
            decay = jnp.exp(totals_ref[j, direction:direction + 1, :]).T
            joined = decay * state + states_ref[
                j, direction * width:(direction + 1) * width, :].astype(f32)
            ahead = place < j if direction == 1 else place > j
            state = jnp.where(ahead, joined, state)
        mixture = mixture + dot(qc_ref[:, direction * width:(direction + 1) * width],
                                state.astype(bf16))
    if final:
        squares = jnp.mean(mixture * mixture, axis=1, keepdims=True)
        gate = gate_ref[...].astype(f32)
        normed = mixture * lax.rsqrt(squares + norm_eps) * gain_ref[...]
        result_ref[...] = (normed * (gate / (1.0 + jnp.exp(-gate)))).astype(bf16)
    else:
        result_ref[...] = mixture


def call(kernel, out_shape, *args):
    return pl.pallas_call(
        kernel,
        out_shape=out_shape,
        in_specs=[pl.BlockSpec(memory_space=pltpu.VMEM)] * len(args),
        out_specs=jax.tree.map(lambda _: pl.BlockSpec(memory_space=pltpu.VMEM), out_shape),
        compiler_params=pltpu.CompilerParams(vmem_limit_bytes=48 * 1024 * 1024),
        cost_estimate=pl.CostEstimate(flops=4_000_000_000, bytes_accessed=4_000_000,
                                      transcendentals=1_000_000),
    )(*args)


def project(rows, weight):
    return jnp.dot(rows, weight, preferred_element_type=f32).astype(bf16)


def body(
    latent,
    context,
    condition,
    context_condition,
    mod_weight,
    mod_bias,
    query_weight,
    key_weight,
    value_weight,
    out_gate_weight,
    decay_in_weight,
    decay_weight,
    decay_bias,
    extra_decay,
    norm_gain,
    out_weight,
    final_gain,
    final_bias,
):
    model_width = latent.shape[1]
    head_keys = query_weight.shape[1] // ATTENTION_HEADS
    value_cols = value_weight.shape[1]
    tp_index = lax.axis_index("tp")
    sp_index = lax.axis_index("sp")
    head_share = lax.axis_size("tp") // ATTENTION_HEADS
    head_index = tp_index // head_share
    part_index = tp_index % head_share
    key_start = head_index * head_keys

    own_qk = jnp.concatenate(
        [lax.dynamic_slice_in_dim(w, key_start, head_keys, 1) for w in (query_weight, key_weight)],
        axis=1,
    )
    activated = jax.nn.silu(jnp.stack([condition, context_condition])).astype(bf16)
    partial_value = jnp.dot(activated, mod_weight, preferred_element_type=f32)
    row_sums = lax.psum(partial_value, "sp")
    modulation = lax.all_gather(row_sums, "tp", axis=1, tiled=True)
    modulation = modulation + mod_bias
    shifts = modulation[:, :model_width]
    scales = modulation[:, model_width : 2 * model_width]
    branch_gate = modulation[0, 2 * model_width :]

    qk_head = lax.all_gather(own_qk, "sp", axis=0, tiled=True)
    rows = lax.all_gather(latent, "tp", axis=0, tiled=True)
    mod_context = (context.astype(f32) * (1.0 + scales[1]) + shifts[1]).astype(bf16)
    context_local = jnp.concatenate(
        [
            project(mod_context, qk_head[:, head_keys:]),
            project(mod_context, value_weight),
            project(mod_context, decay_in_weight),
        ],
        axis=1,
    )
    gathered_context = lax.all_gather(context_local, "sp", axis=0, tiled=True)
    mod_latent = (rows.astype(f32) * (1.0 + scales[0]) + shifts[0]).astype(bf16)
    qk = project(mod_latent, qk_head)
    value_rows = project(mod_latent, value_weight)
    out_gate = project(mod_latent, out_gate_weight)
    low_rank = project(mod_latent, decay_in_weight)
    count = rows.shape[0]
    token_places = sp_index * count + jnp.arange(count, dtype=jnp.int32)
    cosine, sine = rope_tables(token_places, head_keys)
    head_bias = lax.dynamic_slice_in_dim(decay_bias, key_start, head_keys, 1)
    head_gate = lax.dynamic_slice_in_dim(decay_weight, key_start, head_keys, 2)
    head_extra = lax.dynamic_index_in_dim(extra_decay, head_index, 1, keepdims=False).T

    sds = jax.ShapeDtypeStruct
    out_local, qc, states, totals = call(
        local_kernel,
        (
            sds((count, value_cols), f32),
            sds((count, 2 * head_keys), bf16),
            sds((2 * head_keys, value_cols), bf16),
            sds((2, head_keys), f32),
        ),
        qk[:, :head_keys], qk[:, head_keys:], value_rows, low_rank, head_extra, head_gate,
        head_bias, cosine, sine,
    )
    start = call(
        context_kernel,
        sds((2, head_keys, value_cols), f32),
        gathered_context[:, :head_keys],
        gathered_context[:, head_keys : head_keys + value_cols],
        gathered_context[:, head_keys + value_cols :],
        head_gate, head_bias,
    )
    all_states = lax.all_gather(states, "sp")
    all_totals = lax.all_gather(totals, "sp")
    place = jnp.full((1, value_cols), sp_index, jnp.int32)
    gain_slice = lax.dynamic_slice_in_dim(norm_gain, part_index * value_cols, value_cols, 0)
    final = head_share == 1
    joined = call(
        functools.partial(join_kernel, final),
        sds((count, value_cols), bf16 if final else f32),
        out_local, qc, all_states, all_totals, start, out_gate, gain_slice[None, :], place,
    )
    if final:
        gated_rows = joined
    else:
        squares = jnp.sum(joined * joined, axis=1)
        onehot = (jnp.arange(ATTENTION_HEADS) == head_index).astype(f32)
        sums = lax.psum(onehot[:, None] * squares[None, :], "tp")
        head_sum = jnp.sum(sums * onehot[:, None], axis=0)
        normed = joined * lax.rsqrt(head_sum / DV + norm_eps)[:, None] * gain_slice
        gated_rows = (normed * jax.nn.silu(out_gate.astype(f32))).astype(bf16)
    full_out = lax.all_gather(out_weight, "tp", axis=0, tiled=True)
    regrouped = lax.all_to_all(gated_rows, "tp", split_axis=0, concat_axis=1, tiled=True)
    branch = jnp.dot(regrouped, full_out, preferred_element_type=f32)
    summed = residual_scale * latent.astype(f32) + branch_gate * branch
    row_mean = jnp.mean(summed, axis=1, keepdims=True)
    centered = summed - row_mean
    variance = jnp.mean(centered * centered, axis=1, keepdims=True)
    return (centered * lax.rsqrt(variance + norm_eps) * final_gain + final_bias).astype(bf16)


def solution(mesh):
    placed = (
        P(("grp", "sp", "tp"), None),
        P(("grp", "sp"), None),
        P(("grp", "sp")),
        P("sp"),
        P("sp", "tp"),
        P(),
        P("sp", None),
        P("sp", None),
        P(None, "tp"),
        P(None, "tp"),
        P(),
        P(),
        P(),
        P(None, None, "sp"),
        P(),
        P("tp", None),
        P(),
        P(),
    )
    return jax.shard_map(
        body, mesh=mesh, in_specs=placed, out_specs=P(("grp", "sp", "tp"), None), check_vma=False
    )
```

time: 407 us -> 234 us (0.57); the launches traced: 401 us -> 233 us
  matrix products: 115 us -> 16.7 us
  local copies, waits for them, and re-layouts: 98.8 us -> 17.2 us
  waiting for transfers between devices: 39.3 us -> 74.4 us
  other arithmetic: 32.2 us -> 5.29 us
  Pallas kernels: 0 us -> 14.1 us
  blocking collectives: 99.8 us -> 91.7 us
    dot_general x76 -> x9, matrix products: 115 us -> 16.7 us  [the longest x7 10.1 us: project(): return jnp.dot(rows, weight, preferred_element_type=f32).astype(bf16)]
    all_gather x6 -> x4, waiting for transfers between devices: 38.8 us -> 73.4 us  [the longest x1 36.5 us: body(): full_out = lax.all_gather(out_weight, 'tp', axis=0, tiled=True)]
    rev x11 -> x0, local copies, waits for them, and re-layouts: 29.5 us -> none  [flip_rows(): return jnp.flip(values, axis=0)]
    another operation x21 -> x0, local copies, waits for them, and re-layouts: 21.9 us -> none
    pallas_call x0 -> x3, Pallas kernels: none -> 14.1 us  [call(): pl.pallas_call(kernel, out_shape=out_shape, in_specs=[pl.BlockSpec(memory...]
    squeeze x16 -> x0, local copies, waits for them, and re-layouts: 13.6 us -> none  [blocked_scan(): lax.scan(advance, start, (blocks(queries), blocks(key_rows), blocks(value...]
    another operation x29 -> x0, other arithmetic: 13.4 us -> none
    unnamed x81 -> x68, local copies, waits for them, and re-layouts: 17.6 us -> 10.2 us
  transfers between devices with their start and end apart: 6 -> 4, of which waited for: 2 -> 3; matrix products, arithmetic and copies ran while one was open for 53% -> 5% of each run, Pallas kernels for 0% -> 3%
where the time goes in v1:
time: 234 us; the launch traced here: 233 us
  blocking collectives  91.7 us (39%)
  waiting for transfers between devices  74.4 us (32%)
  local copies, waits for them, and re-layouts  17.2 us (7%)
  matrix products  16.7 us (7%)
  Pallas kernels  14.1 us (6%)
  between operations  13.5 us (6%)
  other arithmetic  5.29 us (2%)
    all_gather x1, waiting for transfers between devices, body(): full_out = lax.all_gather(out_weight, 'tp', axis=0, tiled=True)  36.5 us
    all_gather x1, blocking collectives, body(): gathered_context = lax.all_gather(context_local, 'sp', axis=0, tiled=True)  33.8 us
    all_gather x1, waiting for transfers between devices, body(): rows = lax.all_gather(latent, 'tp', axis=0, tiled=True)  22.9 us
    psum x1, blocking collectives, body(): row_sums = lax.psum(partial_value, 'sp')  21.3 us
    all_to_all x1, blocking collectives, body(): lax.all_to_all(gated_rows, 'tp', split_axis=0, concat_axis=1, tiled=True)  18.3 us
    pallas_call x3, Pallas kernels, call(): pl.pallas_call(kernel, out_shape=out_shape, in_specs=[pl.BlockSpec(memory...  14.1 us
    all_gather x1, waiting for transfers between devices, body(): qk_head = lax.all_gather(own_qk, 'sp', axis=0, tiled=True)  14 us
    all_gather x1, blocking collectives, body(): all_totals = lax.all_gather(totals, 'sp')  13.1 us
  transfers between devices with their start and end apart: 4, of which 3 were waited for; matrix products, arithmetic and copies ran while one was open for 5% of the time, Pallas kernels for 3%

profile of v1, /device:TPU:0, one launch (start us, length us, event | category | flops | bytes accessed | tf_op | source)
XLA Modules:
  0.0 233.2 jit_solution(3667902116743882174)
XLA Ops:
  6.6 1.2 constant_dynamic-slice_fusion.3
  7.8 0.8 pad_maximum_fusion
  8.6 0.0 all-gather.10.cloned.1.call-update
  8.6 0.0 all-gather.8.cloned.1.call-start
  8.7 0.7 all-gather.8.cloned.1.call-update
  9.4 0.0 all-gather.14.cloned.1.call-start
  9.4 0.7 constant_dynamic-slice_fusion.2
  10.2 0.1 copy.30
  10.3 0.0 copy-done.26
  10.3 0.0 copy-done.25
  10.3 1.7 fusion.5
  12.1 21.3 %psum.7 = f32[2,1536]{1,0:T(2,128)S(1)} all-reduce(f32[2,1536]{1,0:T(2,128)S(1)} %fusion.5), channel_id=1, replica_groups=mesh['grp'=2,'sp'=4,'tp'=4] {'sp'}, use_global_device_ids=true, to_apply=%region_0.1 | all-reduce | flops 3072 | bytes 24576 | tf_op jit(solution)/shard_map/psum | solution.py:214
  33.3 5.2 %all_gather.27 = f32[2,6144]{1,0:T(2,128)S(1)} all-gather(f32[2,1536]{1,0:T(2,128)S(1)} %psum.7), channel_id=1, replica_groups=mesh['grp'=2,'sp'=4,'tp'=4] {'tp'}, dimensions={1}, use_global_device_ids=true | all-gather | bytes 61440 | tf_op jit(solution)/shard_map/all_gather | solution.py:215
  38.5 1.3 constant_dynamic-slice_fusion.db_ref
  39.8 0.7 constant_dynamic-slice_fusion.1.dw_ref
  40.6 1.9 fusion.2
  42.5 0.3 pad_maximum_fusion.1.cos_ref
  42.7 0.3 pad_maximum_fusion.2.sin_ref
  43.1 0.6 fusion.16
  43.7 14.0 %all-gather.10.cloned.1.call-done = bf16[2048,512]{1,0:T(8,128)(2,1)} async-done(((bf16[512,512]{1,0:T(8,128)(2,1)}), bf16[2048,512]{1,0:T(8,128)(2,1)}) %all-gather.10.cloned.1.call-update) | async-done | bytes 2097168 | tf_op jit(solution)/shard_map/all_gather | solution.py:221
  57.7 22.9 %all-gather.8.cloned.1.call-done = bf16[512,2048]{1,0:T(8,128)(2,1)} async-done(((bf16[128,2048]{1,0:T(8,128)(2,1)}), bf16[512,2048]{1,0:T(8,128)(2,1)}) %all-gather.8.cloned.1.call-update) | async-done | bytes 2097168 | tf_op jit(solution)/shard_map/all_gather | solution.py:222
  80.6 3.6 %convolution_convert_fusion.2 = bf16[512,512]{1,0:T(8,128)(2,1)S(1)} fusion(bf16[2048,512]{1,0:T(8,128)(2,1)} %all-gather.10.cloned.1.call-done, bf16[512,2048]{1,0:T(8,128)(2,1)} %all-gather.8.cloned.1.call-done, f32[2048]{0:T(1024)S(1)} %bitcast.33, f32[2048]{0:T(1024)S(1)} %bitcast.37), kind=kOutput, calls=%fused_computation.5 | convolution fusion | flops 1078198272 | bytes 4734976 | tf_op jit(solution)/shard_map/dot_general | solution.py:175
  84.2 0.8 fusion.15
  85.0 0.0 copy-done.32
  85.0 1.3 convolution_convert_fusion.5
  86.4 0.9 copy.31.low_ref
  87.2 0.0 copy-start.1
  87.3 2.9 %convolution_convert_fusion.1.v_ref = bf16[512,512]{1,0:T(8,128)(2,1)S(1)} fusion(bf16[2048,512]{1,0:T(8,128)(2,1)S(1)} %copy-done, bf16[512,2048]{1,0:T(8,128)(2,1)} %all-gather.8.cloned.1.call-done, f32[2048]{0:T(1024)} %bitcast.35, f32[2048]{0:T(1024)} %bitcast.39), kind=kOutput, calls=%fused_computation.4 | convolution fusion | flops 1078198272 | bytes 4734976 | tf_op jit(solution)/shard_map/dot_general | solution.py:175
  90.2 6.4 %shard_map.172 = (f32[512,512]{1,0:T(8,128)S(1)}, bf16[512,512]{1,0:T(8,128)(2,1)S(1)}, bf16[512,512]{1,0:T(8,128)(2,1)}, f32[2,256]{1,0:T(2,128)S(1)}) custom-call(bf16[512,256]{1,0:T(8,128)(2,1)S(1)} %copy-done.2, bf16[512,256]{1,0:T(8,128)(2,1)S(1)} %copy-done.1, bf16[512,512]{1,0:T(8,128)(2,1)S(1)} %convolution_convert_fusion.1.v_ref, ...), custom_call_target="tpu_custom_call" | custom-call | flops 4000000000 | bytes 4000000 | tf_op jit(solution)/shard_map/pallas_call | solution.py:163
  96.6 0.6 copy-done.3
  97.2 1.0 copy-done.9
  98.2 0.8 copy-done.13
  99.1 0.0 all-gather.14.cloned.1.call-update
  99.1 0.2 all-gather.12.cloned.1.call-start
  99.3 0.3 all-gather.12.cloned.1.call-update
  99.7 0.1 copy-done.23
  99.8 0.0 copy-done.24
  99.8 0.4 copy-done.31
  100.1 0.0 copy-done.33
  100.2 0.3 convolution_convert_fusion.6
  100.4 0.1 copy.32
  100.6 0.5 convolution_convert_fusion.3
  101.0 1.1 copy-done.30
  102.1 0.3 convolution_convert_fusion.4
  102.5 33.8 %all_gather.34 = bf16[512,800]{1,0:T(8,128)(2,1)S(1)} all-gather(bf16[128,800]{1,0:T(8,128)(2,1)S(1)} %pad_maximum_fusion.3), channel_id=1, replica_groups=mesh['grp'=2,'sp'=4,'tp'=4] {'sp'}, dimensions={0}, use_global_device_ids=true | all-gather | bytes 1024000 | tf_op jit(solution)/shard_map/all_gather | solution.py:232
  136.4 13.1 %all-gather.2.totals_ref = f32[4,2,256]{2,1,0:T(2,128)S(1)} all-gather(f32[1,2,256]{2,1,0:T(2,128)S(1)} %bitcast.28), channel_id=3, replica_groups=mesh['grp'=2,'sp'=4,'tp'=4] {'sp'}, dimensions={0}, use_global_device_ids=true | all-gather | bytes 10240 | tf_op jit(solution)/shard_map/all_gather | solution.py:266
  149.5 0.0 copy-start.27
  149.5 6.1 %shard_map.173.start_ref = f32[2,256,512]{2,1,0:T(8,128)S(1)} custom-call(bf16[512,256]{1,0:T(8,128)(2,1)S(1)} %slice.58.k_ref, bf16[512,512]{1,0:T(8,128)(2,1)S(1)} %slice.59.v_ref, bf16[512,32]{1,0:T(8,128)(2,1)S(1)} %slice.60.low_ref, bf16[2,16,256]{2,1,0:T(8,128)(2,1)S(1)} %constant_dynamic-slice_fusion.1.dw_ref, f32[2,256]{1,0:T(2,128)S(1)} %copy-done.6), custom_call_target="tpu_custom_call" | custom-call | flops 4000000000 | bytes 4000000 | tf_op jit(solution)/shard_map/pallas_call | solution.py:163
  155.6 0.0 copy-start.11
  155.6 1.0 copy-done.11
  156.6 0.0 copy-start.8
  156.6 1.3 convolution_convert_fusion.gate_ref
  157.9 0.0 all-gather.14.cloned.1.call-done
  157.9 1.6 copy-done.7
  159.5 1.2 copy-done.10
  160.7 1.2 copy-done.12
  162.0 1.1 copy-done.14
  163.1 1.6 shard_map.174
  164.7 1.0 copy.33
  165.7 18.3 %all_to_all.19 = bf16[4,128,512]{1,2,0:T(8,128)(2,1)S(1)} all-to-all(bf16[4,128,512]{1,2,0:T(8,128)(2,1)} %copy.33), channel_id=1, replica_groups=mesh['grp'=2,'sp'=4,'tp'=4] {'tp'}, dimensions={0} | all-to-all | bytes 1048576 | tf_op jit(solution)/shard_map/all_to_all | solution.py:285
  184.0 36.5 %all-gather.12.cloned.1.call-done = bf16[2048,2048]{1,0:T(8,128)(2,1)} async-done(((bf16[512,2048]{1,0:T(8,128)(2,1)}), bf16[2048,2048]{1,0:T(8,128)(2,1)}) %all-gather.12.cloned.1.call-update) | async-done | bytes 8388624 | tf_op jit(solution)/shard_map/all_gather | solution.py:284
  220.5 4.8 %fusion.17 = (f32[128]{0:T(128)S(1)}, f32[128,2048]{1,0:T(8,128)S(1)}) fusion(bf16[128,2048]{0,1:T(8,128)(2,1)S(1)} %bitcast.31, bf16[2048,2048]{1,0:T(8,128)(2,1)} %all-gather.12.cloned.1.call-done, f32[2048]{0:T(1024)S(1)} %bitcast.32, bf16[128,2048]{1,0:T(8,128)(2,1)} %param.18), kind=kOutput, calls=%fused_computation.56 | convolution fusion | flops 1075052416 | bytes 10494464 | tf_op jit(solution)/shard_map/dot_general | solution.py:286
  225.3 0.3 multiply_reduce_fusion
  225.6 1.0 add_convert_fusion.1
  (59 shorter events, 0.2 us)
Async XLA Ops:
  6.5 80.7 %copy-start = (bf16[2048,512]{1,0:T(8,128)(2,1)S(1)}, bf16[2048,512]{1,0:T(8,128)(2,1)}, u32[]{:S(2)}) copy-start(bf16[2048,512]{1,0:T(8,128)(2,1)} %param.26) | copy-start | bytes 6291460
  6.5 3.8 %copy-start.26 = (f32[512]{0:T(512)S(1)}, f32[512]{0:T(512)}, u32[]{:S(2)}) copy-start(f32[512]{0:T(512)} %param.20) | copy-start | bytes 6148
  6.5 3.8 %copy-start.25 = (f32[512]{0:T(512)S(1)}, f32[512]{0:T(512)}, u32[]{:S(2)}) copy-start(f32[512]{0:T(512)} %param.21) | copy-start | bytes 6148
  6.5 51.2 %all-gather.10.cloned.1.call-start = ((), (), s32[]{:S(2)}) async-start(), calls=%async_computation.2 | async-start | bytes 2621440 | tf_op jit(solution)/shard_map/all_gather | solution.py:221
  8.6 71.9 %all-gather.8.cloned.1.call-start = ((), (), s32[]{:S(2)}) async-start(), calls=%async_computation.1 | async-start | bytes 2621440 | tf_op jit(solution)/shard_map/all_gather | solution.py:222
  9.4 148.5 %all-gather.14.cloned.1.call-start = ((), (), s32[]{:S(2)}) async-start(), calls=%async_computation.4 | async-start | bytes 2621440 | tf_op jit(solution)/shard_map/all_gather | solution.py:265
  40.5 2.5 %copy-start.16 = (f32[6144]{0:T(1024)S(1)}, f32[6144]{0:T(1024)}, u32[]{:S(2)}) copy-start(f32[6144]{0:T(1024)} %param.23) | copy-start | bytes 73732
  43.7 41.3 %copy-start.19 = (f32[1,2048]{1,0:T(1,128)}, f32[1,2048]{1,0:T(1,128)S(1)}, u32[]{:S(2)}) copy-start(f32[1,2048]{1,0:T(1,128)S(1)} %get-tuple-element.18) | copy-start | bytes 24580
  43.7 41.3 %copy-start.21 = (f32[1,2048]{1,0:T(1,128)}, f32[1,2048]{1,0:T(1,128)S(1)}, u32[]{:S(2)}) copy-start(f32[1,2048]{1,0:T(1,128)S(1)} %get-tuple-element.19) | copy-start | bytes 24580
  80.6 4.5 %copy-start.28 = (bf16[512,2048]{1,0:T(8,128)(2,1)S(1)}, bf16[512,2048]{1,0:T(8,128)(2,1)}, u32[]{:S(2)}) copy-start(bf16[512,2048]{1,0:T(8,128)(2,1)} %all-gather.8.cloned.1.call-done) | copy-start | bytes 6291460
  80.6 4.5 %copy-start.32 = (bf16[2048,32]{0,1:T(8,128)(2,1)S(1)}, bf16[2048,32]{0,1:T(8,128)(2,1)}, u32[]{:S(2)}) copy-start(bf16[2048,32]{0,1:T(8,128)(2,1)} %param.28) | copy-start | bytes 393220
  87.2 3.0 %copy-start.1 = (bf16[512,256]{1,0:T(8,128)(2,1)S(1)}, bf16[512,256]{1,0:T(8,128)(2,1)}, u32[]{:S(2)}) copy-start(bf16[512,256]{1,0:T(8,128)(2,1)} %get-tuple-element.13.k_ref) | copy-start | bytes 786436
  87.3 3.0 %copy-start.2 = (bf16[512,256]{1,0:T(8,128)(2,1)S(1)}, bf16[512,256]{1,0:T(8,128)(2,1)}, u32[]{:S(2)}) copy-start(bf16[512,256]{1,0:T(8,128)(2,1)} %get-tuple-element.14.q_ref) | copy-start | bytes 786436
  87.3 3.0 %copy-start.5 = (f32[2,256]{1,0:T(2,128)S(1)}, f32[2,256]{1,0:T(2,128)}, u32[]{:S(2)}) copy-start(f32[2,256]{1,0:T(2,128)} %constant_dynamic-slice_fusion.db_ref) | copy-start | bytes 6148
  96.6 0.6 copy-start.3
  97.2 1.0 copy-start.9
  98.2 0.8 copy-start.13
  99.1 0.7 copy-start.23
  99.1 0.7 copy-start.24
  99.1 1.1 copy-start.31
  99.1 1.1 copy-start.33
  99.1 121.4 %all-gather.12.cloned.1.call-start = ((), (), s32[]{:S(2)}) async-start(), calls=%async_computation.3 | async-start | bytes 10485760 | tf_op jit(solution)/shard_map/all_gather | solution.py:284
  100.6 1.6 copy-start.30
  102.5 33.9 %copy-start.4 = (f32[2,256]{1,0:T(2,128)S(1)}, f32[2,256]{1,0:T(2,128)}, u32[]{:S(2)}) copy-start(f32[2,256]{1,0:T(2,128)} %copy-done.3) | copy-start | bytes 6148
  102.5 47.0 %copy-start.6 = (f32[2,256]{1,0:T(2,128)S(1)}, f32[2,256]{1,0:T(2,128)}, u32[]{:S(2)}) copy-start(f32[2,256]{1,0:T(2,128)} %constant_dynamic-slice_fusion.db_ref) | copy-start | bytes 6148
  149.5 7.1 %copy-start.20 = (f32[1,2048]{1,0:T(1,128)S(1)}, f32[1,2048]{1,0:T(1,128)}, u32[]{:S(2)}) copy-start(f32[1,2048]{1,0:T(1,128)} %copy-done.19) | copy-start | bytes 24580
  149.5 7.1 %copy-start.22 = (f32[1,2048]{1,0:T(1,128)S(1)}, f32[1,2048]{1,0:T(1,128)}, u32[]{:S(2)}) copy-start(f32[1,2048]{1,0:T(1,128)} %copy-done.21) | copy-start | bytes 24580
  149.5 7.1 %copy-start.27 = (bf16[2048,512]{1,0:T(8,128)(2,1)S(1)}, bf16[2048,512]{1,0:T(8,128)(2,1)}, u32[]{:S(2)}) copy-start(bf16[2048,512]{1,0:T(8,128)(2,1)} %param.27) | copy-start | bytes 6291460
  149.5 7.1 %copy-start.29 = (bf16[512,2048]{1,0:T(8,128)(2,1)S(1)}, bf16[512,2048]{1,0:T(8,128)(2,1)}, u32[]{:S(2)}) copy-start(bf16[512,2048]{1,0:T(8,128)(2,1)} %all-gather.8.cloned.1.call-done) | copy-start | bytes 6291460
  155.6 1.0 copy-start.11
  156.6 1.3 copy-start.8
  157.9 1.6 copy-start.7
  159.5 1.2 copy-start.10
  160.7 1.2 copy-start.12
  162.0 1.1 copy-start.14
  164.7 55.8 %copy-start.15 = (f32[1,2048]{1,0:T(1,128)S(1)}, f32[1,2048]{1,0:T(1,128)}, u32[]{:S(2)}) copy-start(f32[1,2048]{1,0:T(1,128)} %get-tuple-element.15) | copy-start | bytes 24580
  220.5 5.1 %copy-start.17 = (f32[2048]{0:T(1024)S(1)}, f32[2048]{0:T(1024)}, u32[]{:S(2)}) copy-start(f32[2048]{0:T(1024)} %param.35) | copy-start | bytes 24580
  220.5 5.1 %copy-start.18 = (f32[2048]{0:T(1024)S(1)}, f32[2048]{0:T(1024)}, u32[]{:S(2)}) copy-start(f32[2048]{0:T(1024)} %param.34) | copy-start | bytes 24580
Sparse Core Ops, SparseCore 0:
  8.9 48.7 all-gather.9
  59.3 21.2 all-gather.7
  99.2 57.7 all-gather.13
  158.4 62.0 all-gather.11

commit v2 on v1

--- a/solution.py
+++ b/solution.py
@@ -171,6 +171,246 @@
     )(*args)
 
 
+MESH = pl.DeviceIdType.MESH
+
+
+def remote(src, dst, send_sem, recv_sem, axis, target):
+    return pltpu.make_async_remote_copy(
+        src_ref=src, dst_ref=dst, send_sem=send_sem, recv_sem=recv_sem,
+        device_id={axis: target}, device_id_type=MESH)
+
+
+class Line:
+    def __init__(self, place, count, axis, target_of, view, chunks, send_sem, recv_sem):
+        self.place, self.count, self.axis, self.target_of = place, count, axis, target_of
+        self.view, self.chunks, self.send_sem, self.recv_sem = view, chunks, send_sem, recv_sem
+
+    def copy(self, way, hop, chunk, block, target):
+        ref = self.view(block, chunk)
+        return remote(ref, ref, self.send_sem.at[way, hop, chunk],
+                      self.recv_sem.at[way, hop, chunk], self.axis, self.target_of(target))
+
+    def outgoing(self, way, hop):
+        place, count = self.place, self.count
+        if way == 0:
+            return place - hop, place + 1, jnp.logical_and(place >= hop, place < count - 1)
+        return place + hop, place - 1, jnp.logical_and(place + hop < count, place > 0)
+
+    def each_send(self, way, hop, chunk, act):
+        block, target, valid = self.outgoing(way, hop)
+
+        @pl.when(valid)
+        def _():
+            act(self.copy(way, hop, chunk, block, target))
+
+    def send(self, way, hop, chunk):
+        self.each_send(way, hop, chunk, lambda c: c.start())
+
+    def drain(self):
+        for way in range(2):
+            for hop in range(self.count - 1):
+                for chunk in range(self.chunks):
+                    self.each_send(way, hop, chunk, lambda c: c.wait_send())
+
+    def arrive(self, way, hop, chunk, then=None):
+        if way == 0:
+            block, source, valid = self.place - 1 - hop, self.place - 1, self.place > hop
+        else:
+            block, source = self.place + 1 + hop, self.place + 1
+            valid = self.place + 1 + hop < self.count
+
+        @pl.when(valid)
+        def _():
+            self.copy(way, hop, chunk, block, source).wait_recv()
+            if then is not None:
+                then(block)
+
+    def forward(self, hop, then=None):
+        for chunk in range(self.chunks):
+            for way in range(2):
+                self.arrive(way, hop, chunk, None if then is None else functools.partial(then, way))
+                if hop + 1 < self.count - 1:
+                    self.send(way, hop + 1, chunk)
+
+
+def open_kernel(partners):
+    barrier = pltpu.get_barrier_semaphore()
+    for axis, target in partners:
+        pl.semaphore_signal(barrier, inc=1, device_id={axis: target}, device_id_type=MESH)
+    return lambda: pl.semaphore_wait(barrier, len(partners))
+
+
+def others(axis):
+    count, place = lax.axis_size(axis), lax.axis_index(axis)
+    return [lax.rem(place + k, count) for k in range(1, count)]
+
+
+def sources(axis):
+    count, place = lax.axis_size(axis), lax.axis_index(axis)
+    return [lax.rem(place + count - k, count) for k in range(1, count)]
+
+
+def spread(buffer, axis, send_sem, recv_sem):
+    place = lax.axis_index(axis)
+    for k, target in enumerate(others(axis)):
+        remote(buffer.at[place], buffer.at[place], send_sem.at[k], recv_sem.at[k],
+               axis, target).start()
+
+
+def spread_arrive(buffer, axis, send_sem, recv_sem):
+    for k, source in enumerate(sources(axis)):
+        remote(buffer.at[source], buffer.at[source], send_sem.at[k], recv_sem.at[k],
+               axis, source).wait_recv()
+
+
+def spread_drain(buffer, axis, send_sem, recv_sem):
+    place = lax.axis_index(axis)
+    for k, target in enumerate(others(axis)):
+        remote(buffer.at[place], buffer.at[place], send_sem.at[k], recv_sem.at[k],
+               axis, target).wait_send()
+
+
+def enter_kernel(chunks, latent_ref, context_ref, cond_ref, mw_ref, mb_ref, qw_ref, kw_ref,
+                 ml_ref, mc_ref, gate_ref, qk_ref,
+                 rows_ref, part_ref, sums_ref, zs, zr, xs, xr, cs, cr, ps, pr, ss, sr):
+    sp, sp_count = lax.axis_index("sp"), lax.axis_size("sp")
+    tp, tp_count = lax.axis_index("tp"), lax.axis_size("tp")
+    own, model_width = latent_ref.shape
+    depth = qw_ref.shape[0]
+    head_keys = qk_ref.shape[1] // 2
+    ready = open_kernel([("sp", t) for t in others("sp")] + [("tp", t) for t in others("tp")])
+    v = cond_ref[...]
+    activated = (v / (1.0 + jnp.exp(-v))).astype(bf16)
+    part_ref[sp] = dot(activated, mw_ref[...])
+    columns = pl.ds(pl.multiple_of((tp // (tp_count // ATTENTION_HEADS)) * head_keys, head_keys),
+                    head_keys)
+    qk_rows = pl.ds(pl.multiple_of(sp * depth, depth), depth)
+    qk_ref[qk_rows, :head_keys] = qw_ref[:, columns]
+    qk_ref[qk_rows, head_keys:] = kw_ref[:, columns]
+    rows_ref[pl.ds(pl.multiple_of(tp * own, own), own), :] = latent_ref[...]
+
+    step = depth // chunks
+    z_line = Line(
+        sp, sp_count, "sp", lambda p: p,
+        lambda block, chunk: qk_ref.at[
+            pl.ds(pl.multiple_of(block * depth + chunk * step, step), step), :],
+        chunks, zs, zr)
+    x_count = tp_count // 2
+    x, core = tp // 2, tp % 2
+
+    def rows_of(block, chunk):
+        return rows_ref.at[pl.ds(pl.multiple_of((2 * block + core) * own, own), own), :]
+
+    x_line = Line(x, x_count, "tp", lambda p: 2 * p + core, rows_of, 1, xs, xr)
+    sibling = tp + 1 - 2 * core
+
+    def cross(block, slot, other=False):
+        side = 1 - core if other else core
+        ref = rows_ref.at[pl.ds(pl.multiple_of((2 * block + side) * own, own), own), :]
+        return remote(ref, ref, cs.at[slot], cr.at[slot], "tp", sibling)
+
+    def slot_of(way, hop):
+        return 1 + way * (x_count - 1) + hop
+
+    ready()
+    spread(part_ref, "sp", ps, pr)
+    for way in range(2):
+        x_line.send(way, 0, 0)
+    cross(x, 0).start()
+    for chunk in range(chunks):
+        for way in range(2):
+            z_line.send(way, 0, chunk)
+    spread_arrive(part_ref, "sp", ps, pr)
+    total = part_ref[0]
+    for j in range(1, sp_count):
+        total = total + part_ref[j]
+    sums_ref[tp] = total
+    spread(sums_ref, "tp", ss, sr)
+    z_line.forward(0)
+    for hop in range(x_count - 1):
+        x_line.forward(hop, lambda way, block, hop=hop: cross(block, slot_of(way, hop)).start())
+    if sp_count > 2:
+        z_line.forward(1)
+    spread_arrive(sums_ref, "tp", ss, sr)
+    modulation = jnp.concatenate([sums_ref[j] for j in range(tp_count)], axis=1) + mb_ref[...]
+    shifts = modulation[:, :model_width]
+    scales = modulation[:, model_width:2 * model_width]
+    gate_ref[...] = modulation[0:1, 2 * model_width:]
+    mc_ref[...] = (context_ref[...].astype(f32) * (1.0 + scales[1:2]) + shifts[1:2]).astype(bf16)
+
+    def each_cross(act_own, act_line):
+        act_own()
+        for way in range(2):
+            for hop in range(x_count - 1):
+                block = x - 1 - hop if way == 0 else x + 1 + hop
+                valid = x > hop if way == 0 else x + 1 + hop < x_count
+
+                @pl.when(valid)
+                def _():
+                    act_line(block, slot_of(way, hop))
+
+    each_cross(lambda: cross(x, 0, True).wait_recv(),
+               lambda block, slot: cross(block, slot, True).wait_recv())
+    for j in range(tp_count):
+        rows = slice(j * own, (j + 1) * own)
+        ml_ref[rows, :] = (rows_ref[rows, :].astype(f32) * (1.0 + scales[0:1])
+                           + shifts[0:1]).astype(bf16)
+    for hop in range(2, sp_count - 1):
+        z_line.forward(hop)
+    each_cross(lambda: cross(x, 0).wait_send(),
+               lambda block, slot: cross(block, slot).wait_send())
+    spread_drain(part_ref, "sp", ps, pr)
+    spread_drain(sums_ref, "tp", ss, sr)
+    x_line.drain()
+    z_line.drain()
+
+
+def comm_call(kernel, out_shape, scratch, collective_id, *args):
+    return pl.pallas_call(
+        kernel,
+        out_shape=out_shape,
+        in_specs=[pl.BlockSpec(memory_space=pltpu.VMEM)] * len(args),
+        out_specs=jax.tree.map(lambda _: pl.BlockSpec(memory_space=pltpu.VMEM), out_shape),
+        scratch_shapes=scratch,
+        compiler_params=pltpu.CompilerParams(
+            vmem_limit_bytes=48 * 1024 * 1024, collective_id=collective_id,
+            has_side_effects=True),
+        cost_estimate=pl.CostEstimate(flops=20_000_000_000, bytes_accessed=60_000_000,
+                                      transcendentals=1_000_000),
+    )(*args)
+
+
+def enter(latent, context, cond, mod_weight, mod_bias, query_weight, key_weight):
+    sp_count, tp_count = lax.axis_size("sp"), lax.axis_size("tp")
+    own, model_width = latent.shape
+    depth = query_weight.shape[0]
+    head_keys = query_weight.shape[1] // ATTENTION_HEADS
+    chunks = 4
+    sds = jax.ShapeDtypeStruct
+    dma = pltpu.SemaphoreType.DMA
+    x_hops = tp_count // 2 - 1
+    return comm_call(
+        functools.partial(enter_kernel, chunks),
+        (
+            sds((own * tp_count, model_width), bf16),
+            sds(context.shape, bf16),
+            sds((1, model_width), f32),
+            sds((depth * sp_count, 2 * head_keys), bf16),
+        ),
+        [
+            pltpu.VMEM((own * tp_count, model_width), bf16),
+            pltpu.VMEM((sp_count, 2, mod_weight.shape[1]), f32),
+            pltpu.VMEM((tp_count, 2, mod_weight.shape[1]), f32),
+            dma((2, sp_count - 1, chunks)), dma((2, sp_count - 1, chunks)),
+            dma((2, x_hops, 1)), dma((2, x_hops, 1)),
+            dma((1 + 2 * x_hops,)), dma((1 + 2 * x_hops,)),
+            dma((sp_count - 1,)), dma((sp_count - 1,)),
+            dma((tp_count - 1,)), dma((tp_count - 1,)),
+        ],
+        1, latent, context, cond, mod_weight, mod_bias[None, :], query_weight, key_weight,
+    )
+
+
 def project(rows, weight):
     return jnp.dot(rows, weight, preferred_element_type=f32).astype(bf16)
 
@@ -195,7 +435,6 @@
     final_gain,
     final_bias,
 ):
-    model_width = latent.shape[1]
     head_keys = query_weight.shape[1] // ATTENTION_HEADS
     value_cols = value_weight.shape[1]
     tp_index = lax.axis_index("tp")
@@ -205,22 +444,11 @@
     part_index = tp_index % head_share
     key_start = head_index * head_keys
 
-    own_qk = jnp.concatenate(
-        [lax.dynamic_slice_in_dim(w, key_start, head_keys, 1) for w in (query_weight, key_weight)],
-        axis=1,
-    )
-    activated = jax.nn.silu(jnp.stack([condition, context_condition])).astype(bf16)
-    partial_value = jnp.dot(activated, mod_weight, preferred_element_type=f32)
-    row_sums = lax.psum(partial_value, "sp")
-    modulation = lax.all_gather(row_sums, "tp", axis=1, tiled=True)
-    modulation = modulation + mod_bias
-    shifts = modulation[:, :model_width]
-    scales = modulation[:, model_width : 2 * model_width]
-    branch_gate = modulation[0, 2 * model_width :]
-
-    qk_head = lax.all_gather(own_qk, "sp", axis=0, tiled=True)
-    rows = lax.all_gather(latent, "tp", axis=0, tiled=True)
-    mod_context = (context.astype(f32) * (1.0 + scales[1]) + shifts[1]).astype(bf16)
+    full_out = lax.all_gather(out_weight, "tp", axis=0, tiled=True)
+    mod_latent, mod_context, branch_gate, qk_head = enter(
+        latent, context, jnp.stack([condition, context_condition]), mod_weight, mod_bias,
+        query_weight, key_weight,
+    )
     context_local = jnp.concatenate(
         [
             project(mod_context, qk_head[:, head_keys:]),
@@ -230,12 +458,11 @@
         axis=1,
     )
     gathered_context = lax.all_gather(context_local, "sp", axis=0, tiled=True)
-    mod_latent = (rows.astype(f32) * (1.0 + scales[0]) + shifts[0]).astype(bf16)
     qk = project(mod_latent, qk_head)
     value_rows = project(mod_latent, value_weight)
     out_gate = project(mod_latent, out_gate_weight)
     low_rank = project(mod_latent, decay_in_weight)
-    count = rows.shape[0]
+    count = mod_latent.shape[0]
     token_places = sp_index * count + jnp.arange(count, dtype=jnp.int32)
     cosine, sine = rope_tables(token_places, head_keys)
     head_bias = lax.dynamic_slice_in_dim(decay_bias, key_start, head_keys, 1)
@@ -262,6 +489,7 @@
         gathered_context[:, head_keys + value_cols :],
         head_gate, head_bias,
     )
+    states, totals, full_out = lax.optimization_barrier((states, totals, full_out))
     all_states = lax.all_gather(states, "sp")
     all_totals = lax.all_gather(totals, "sp")
     place = jnp.full((1, value_cols), sp_index, jnp.int32)
@@ -281,7 +509,6 @@
         head_sum = jnp.sum(sums * onehot[:, None], axis=0)
         normed = joined * lax.rsqrt(head_sum / DV + norm_eps)[:, None] * gain_slice
         gated_rows = (normed * jax.nn.silu(out_gate.astype(f32))).astype(bf16)
-    full_out = lax.all_gather(out_weight, "tp", axis=0, tiled=True)
     regrouped = lax.all_to_all(gated_rows, "tp", split_axis=0, concat_axis=1, tiled=True)
     branch = jnp.dot(regrouped, full_out, preferred_element_type=f32)
     summed = residual_scale * latent.astype(f32) + branch_gate * branch

time: 234 us -> 170 us (0.73)
  waiting for transfers between devices: 74.4 us -> 4.67 us
  Pallas kernels: 14.1 us -> 56.5 us
  blocking collectives: 91.7 us -> 55.9 us
    pallas_call x0 -> x1, Pallas kernels: none -> 43.2 us  [comm_call(): pl.pallas_call(kernel, out_shape=out_shape, in_specs=[pl.BlockSpec(memory...]
    all_gather x2 -> x0, waiting for transfers between devices: 36.9 us -> none  [the longest x1 22.9 us: body(): rows = lax.all_gather(latent, 'tp', axis=0, tiled=True)]
    all_gather x1, waiting for transfers between devices: 36.5 us -> 2.54 us  [body(): full_out = lax.all_gather(out_weight, 'tp', axis=0, tiled=True)]
    psum x1 -> x0, blocking collectives: 21.3 us -> none  [body(): row_sums = lax.psum(partial_value, 'sp')]
    all_to_all x1, blocking collectives: 18.3 us -> 12.3 us  [body(): lax.all_to_all(gated_rows, 'tp', split_axis=0, concat_axis=1, tiled=True)]
    all_gather x1 -> x0, blocking collectives: 5.2 us -> none  [body(): modulation = lax.all_gather(row_sums, 'tp', axis=1, tiled=True)]
    unnamed x68 -> x64, local copies, waits for them, and re-layouts: 10.2 us -> 14.8 us
    all_gather x1, blocking collectives: 33.8 us -> 31 us  [body(): gathered_context = lax.all_gather(context_local, 'sp', axis=0, tiled=True)]
  transfers between devices with their start and end apart: 4 -> 2, of which waited for: 3 -> 2; matrix products, arithmetic and copies ran while one was open for 5% -> 10% of each run, Pallas kernels for 3% -> 32%
where the time goes in v2:
time: 170 us; the launch traced here: 169 us
  Pallas kernels  56.5 us (33%)
  blocking collectives  55.9 us (33%)
  local copies, waits for them, and re-layouts  19.3 us (11%)
  matrix products  15.4 us (9%)
  between operations  13.8 us (8%)
  waiting for transfers between devices  4.67 us (3%)
  other arithmetic  3.81 us (2%)
    pallas_call x1, Pallas kernels, comm_call(): pl.pallas_call(kernel, out_shape=out_shape, in_specs=[pl.BlockSpec(memory...  43.2 us
    all_gather x1, blocking collectives, body(): gathered_context = lax.all_gather(context_local, 'sp', axis=0, tiled=True)  31 us
    unnamed x64, local copies, waits for them, and re-layouts  14.8 us
    pallas_call x3, Pallas kernels, call(): pl.pallas_call(kernel, out_shape=out_shape, in_specs=[pl.BlockSpec(memory...  13.3 us
    all_gather x1, blocking collectives, body(): all_totals = lax.all_gather(totals, 'sp')  12.7 us
    all_to_all x1, blocking collectives, body(): lax.all_to_all(gated_rows, 'tp', split_axis=0, concat_axis=1, tiled=True)  12.3 us
    dot_general x7, matrix products, project(): return jnp.dot(rows, weight, preferred_element_type=f32).astype(bf16)  10.6 us
    dot_general x1, matrix products, body(): branch = jnp.dot(regrouped, full_out, preferred_element_type=f32)  4.79 us
  transfers between devices with their start and end apart: 2, of which 2 were waited for; matrix products, arithmetic and copies ran while one was open for 10% of the time, Pallas kernels for 32%

profile of v2, /device:TPU:0, one launch (start us, length us, event | category | flops | bytes accessed | tf_op | source)
XLA Modules:
  0.0 169.5 jit_solution(9268698283201737938)
XLA Ops:
  6.5 0.0 copy-start
  6.5 0.0 all-gather.6.cloned.1.call-start
  6.6 0.7 all-gather.6.cloned.1.call-update
  7.3 0.0 all-gather.8.cloned.1.call-start
  7.3 0.8 constant_dynamic-slice_fusion.2
  8.1 0.1 copy.30
  8.2 0.0 copy-done.28
  8.3 0.0 copy-done.29
  8.3 0.0 copy-done.1
  8.3 0.0 copy-done.14
  8.3 0.0 copy-start.10
  8.3 1.4 copy-done.10
  9.7 1.2 copy-done.11
  10.9 1.2 copy-done.12
  12.2 1.0 copy-done.13
  13.2 43.2 %shard_map.172 = (bf16[512,2048]{1,0:T(8,128)(2,1)}, bf16[128,2048]{1,0:T(8,128)(2,1)S(1)}, f32[1,2048]{1,0:T(1,128)S(1)}, bf16[2048,512]{1,0:T(8,128)(2,1)}) custom-call(bf16[128,2048]{1,0:T(8,128)(2,1)S(1)} %copy-done.1, bf16[128,2048]{1,0:T(8,128)(2,1)S(1)} %copy-done.13, f32[2,512]{1,0:T(2,128)S(1)} %pad_maximum_fusion.3.cond_ref, ...), custom_call_target="tpu_custom_call" | custom-call | flops 20000000000 | bytes 60000000 | tf_op jit(solution)/shard_map/pallas_call | solution.py:369
  56.4 0.0 copy-start.3
  56.4 0.6 copy-done.3
  57.0 0.0 copy-done.25
  57.0 2.9 %convolution_convert_fusion.5 = bf16[512,32]{0,1:T(8,128)(2,1)} fusion(bf16[512,2048]{1,0:T(8,128)(2,1)} %get-tuple-element.17, bf16[2048,32]{0,1:T(8,128)(2,1)S(1)} %copy-done.25), kind=kOutput, calls=%fused_computation.7 | convolution fusion | flops 67125248 | bytes 2260992 | tf_op jit(solution)/shard_map/dot_general | solution.py:415
  60.0 0.9 copy.31.low_ref
  60.9 0.7 constant_dynamic-slice_fusion.db_ref
  61.6 0.7 constant_dynamic-slice_fusion.1.dw_ref
  62.3 1.9 %fusion.2 = (f32[512,64]{1,0:T(8,128)S(1)}, f32[512,64]{1,0:T(8,128)S(1)}, f32[512,64]{1,0:T(8,128)S(1)}, f32[512,64]{1,0:T(8,128)S(1)}, f32[512,64]{1,0:T(8,128)S(1)}, /*index=5*/f32[512,64]{1,0:T(8,128)S(1)}) fusion(f32[64]{0:T(128)S(1)} %multiply_power_fusion, f32[512]{0:T(512)S(1)} %get-tuple-element.40, f32[512]{0:T(512)S(1)} %get-tuple-element.41), kind=kLoop, calls=%fused_computation.19 | loop fusion | flops 131072 | bytes 790784 | tf_op jit(solution)/shard_map/neg | solution.py:32
  64.2 0.3 pad_maximum_fusion.cos_ref
  64.5 0.3 pad_maximum_fusion.1.sin_ref
  64.8 1.2 convolution_convert_fusion.2
  66.1 1.2 convolution_convert_fusion.1.v_ref
  67.3 5.6 %shard_map.173 = (f32[512,512]{1,0:T(8,128)S(1)}, bf16[512,512]{1,0:T(8,128)(2,1)S(1)}, bf16[512,512]{1,0:T(8,128)(2,1)S(1)}, f32[2,256]{1,0:T(2,128)S(1)}) custom-call(bf16[512,256]{1,0:T(8,128)(2,1)S(1)} %get-tuple-element.28.q_ref, bf16[512,256]{1,0:T(8,128)(2,1)S(1)} %get-tuple-element.27.k_ref, bf16[512,512]{1,0:T(8,128)(2,1)S(1)} %convolution_convert_fusion.1.v_ref, ...), custom_call_target="tpu_custom_call" | custom-call | flops 4000000000 | bytes 4000000 | tf_op jit(solution)/shard_map/pallas_call | solution.py:163
  73.0 0.8 copy-done.2
  73.8 0.6 copy-done.5
  74.4 1.0 copy-done.17
  75.3 0.8 copy-done.21
  76.1 2.5 %all-gather.6.cloned.1.call-done = bf16[2048,2048]{1,0:T(8,128)(2,1)} async-done(((bf16[512,2048]{1,0:T(8,128)(2,1)}), bf16[2048,2048]{1,0:T(8,128)(2,1)}) %all-gather.6.cloned.1.call-update) | async-done | bytes 8388624 | tf_op jit(solution)/shard_map/all_gather | solution.py:447
  78.7 0.0 all-gather.8.cloned.1.call-update
  78.7 1.2 convolution_convert_fusion.6
  79.9 0.1 copy.32
  80.0 1.5 convolution_convert_fusion.4
  81.6 0.5 convolution_convert_fusion.3
  82.0 0.0 copy-start.8
  82.1 31.0 %all_gather.23 = bf16[512,800]{1,0:T(8,128)(2,1)S(1)} all-gather(bf16[128,800]{1,0:T(8,128)(2,1)S(1)} %pad_maximum_fusion.2), channel_id=1, replica_groups=mesh['grp'=2,'sp'=4,'tp'=4] {'sp'}, dimensions={0}, use_global_device_ids=true | all-gather | bytes 1024000 | tf_op jit(solution)/shard_map/all_gather | solution.py:460
  113.2 0.0 copy-start.30
  113.2 6.1 %shard_map.174.start_ref = f32[2,256,512]{2,1,0:T(8,128)S(1)} custom-call(bf16[512,256]{1,0:T(8,128)(2,1)S(1)} %slice.26.k_ref, bf16[512,512]{1,0:T(8,128)(2,1)S(1)} %slice.27.v_ref, bf16[512,32]{1,0:T(8,128)(2,1)S(1)} %slice.28.low_ref, bf16[2,16,256]{2,1,0:T(8,128)(2,1)S(1)} %constant_dynamic-slice_fusion.1.dw_ref, f32[2,256]{1,0:T(2,128)S(1)} %copy-done.8), custom_call_target="tpu_custom_call" | custom-call | flops 4000000000 | bytes 4000000 | tf_op jit(solution)/shard_map/pallas_call | solution.py:163
  119.3 0.0 copy-done.24
  119.3 0.0 copy-done.30
  119.3 0.0 copy-start.19
  119.3 0.0 copy-start.6
  119.3 0.0 copy-start.15
  119.3 2.0 %convolution_convert_fusion.gate_ref = bf16[512,512]{1,0:T(8,128)(2,1)} fusion(bf16[512,2048]{1,0:T(8,128)(2,1)S(1)} %copy-done.24, bf16[2048,512]{1,0:T(8,128)(2,1)S(1)} %copy-done.30), kind=kOutput, calls=%fused_computation.2 | convolution fusion | flops 1074003968 | bytes 4718592 | tf_op jit(solution)/shard_map/dot_general | solution.py:415
  121.3 0.0 copy-done.19
  121.3 12.7 %all-gather.2.totals_ref = f32[4,2,256]{2,1,0:T(2,128)S(1)} all-gather(f32[1,2,256]{2,1,0:T(2,128)S(1)} %bitcast.32), channel_id=3, replica_groups=mesh['grp'=2,'sp'=4,'tp'=4] {'sp'}, dimensions={0}, use_global_device_ids=true | all-gather | bytes 10240 | tf_op jit(solution)/shard_map/all_gather | solution.py:494
  134.0 1.4 all-gather.8.cloned.1.call-done
  135.5 1.6 copy-done.9
  137.1 1.0 copy-done.16
  138.1 1.2 copy-done.18
  139.3 1.2 copy-done.20
  140.6 1.0 copy-done.22
  141.6 1.6 shard_map.175
  143.2 0.0 copy-start.4
  143.2 1.0 copy.33
  144.2 12.3 %all_to_all.19 = bf16[4,128,512]{1,2,0:T(8,128)(2,1)S(1)} all-to-all(bf16[4,128,512]{1,2,0:T(8,128)(2,1)} %copy.33), channel_id=1, replica_groups=mesh['grp'=2,'sp'=4,'tp'=4] {'tp'}, dimensions={0} | all-to-all | bytes 1048576 | tf_op jit(solution)/shard_map/all_to_all | solution.py:512
  156.5 4.8 %fusion.10 = (f32[128]{0:T(128)S(1)}, f32[128,2048]{1,0:T(8,128)S(1)}) fusion(bf16[128,2048]{0,1:T(8,128)(2,1)S(1)} %bitcast.36, bf16[2048,2048]{1,0:T(8,128)(2,1)} %all-gather.6.cloned.1.call-done, f32[2048]{0:T(1024)S(1)} %bitcast.31, bf16[128,2048]{1,0:T(8,128)(2,1)S(1)} %copy-done.1), kind=kOutput, calls=%fused_computation.41 | convolution fusion | flops 1075052416 | bytes 10494464 | tf_op jit(solution)/shard_map/dot_general | solution.py:513
  161.3 0.3 multiply_reduce_fusion
  161.6 1.0 add_convert_fusion
  (44 shorter events, 0.2 us)
Async XLA Ops:
  6.5 59.5 %copy-start = (bf16[2048,512]{1,0:T(8,128)(2,1)S(1)}, bf16[2048,512]{1,0:T(8,128)(2,1)}, u32[]{:S(2)}) copy-start(bf16[2048,512]{1,0:T(8,128)(2,1)} %param.26) | copy-start | bytes 6291460
  6.5 1.7 %copy-start.28 = (f32[512]{0:T(512)S(1)}, f32[512]{0:T(512)}, u32[]{:S(2)}) copy-start(f32[512]{0:T(512)} %param.21) | copy-start | bytes 6148
  6.5 1.7 %copy-start.29 = (f32[512]{0:T(512)S(1)}, f32[512]{0:T(512)}, u32[]{:S(2)}) copy-start(f32[512]{0:T(512)} %param.20) | copy-start | bytes 6148
  6.5 1.7 %copy-start.1 = (bf16[128,2048]{1,0:T(8,128)(2,1)S(1)}, bf16[128,2048]{1,0:T(8,128)(2,1)}, u32[]{:S(2)}) copy-start(bf16[128,2048]{1,0:T(8,128)(2,1)} %latent_ref.1) | copy-start | bytes 1572868
  6.5 1.8 %copy-start.14 = (f32[6144]{0:T(1024)S(1)}, f32[6144]{0:T(1024)}, u32[]{:S(2)}) copy-start(f32[6144]{0:T(1024)} %param.23) | copy-start | bytes 73732
  6.5 72.1 %all-gather.6.cloned.1.call-start = ((), (), s32[]{:S(2)}) async-start(), calls=%async_computation.1 | async-start | bytes 10485760 | tf_op jit(solution)/shard_map/all_gather | solution.py:447
  7.3 128.2 %all-gather.8.cloned.1.call-start = ((), (), s32[]{:S(2)}) async-start(), calls=%async_computation.2 | async-start | bytes 2621440 | tf_op jit(solution)/shard_map/all_gather | solution.py:493
  8.3 1.4 copy-start.10
  9.7 1.2 copy-start.11
  10.9 1.2 copy-start.12
  12.2 1.0 copy-start.13
  13.2 43.8 %copy-start.25 = (bf16[2048,32]{0,1:T(8,128)(2,1)S(1)}, bf16[2048,32]{0,1:T(8,128)(2,1)}, u32[]{:S(2)}) copy-start(bf16[2048,32]{0,1:T(8,128)(2,1)} %param.28) | copy-start | bytes 393220
  56.4 0.6 copy-start.3
  61.6 5.8 %copy-start.7 = (f32[2,256]{1,0:T(2,128)}, f32[2,256]{1,0:T(2,128)S(1)}, u32[]{:S(2)}) copy-start(f32[2,256]{1,0:T(2,128)S(1)} %constant_dynamic-slice_fusion.db_ref) | copy-start | bytes 6148
  62.3 2.5 %copy-start.23 = (bf16[512,2048]{1,0:T(8,128)(2,1)S(1)}, bf16[512,2048]{1,0:T(8,128)(2,1)}, u32[]{:S(2)}) copy-start(bf16[512,2048]{1,0:T(8,128)(2,1)} %get-tuple-element.17) | copy-start | bytes 6291460
  62.3 2.5 %copy-start.31 = (bf16[2048,512]{1,0:T(8,128)(2,1)S(1)}, bf16[2048,512]{1,0:T(8,128)(2,1)}, u32[]{:S(2)}) copy-start(bf16[2048,512]{1,0:T(8,128)(2,1)} %get-tuple-element.18) | copy-start | bytes 6291460
  72.9 0.8 copy-start.2
  73.8 0.6 copy-start.5
  74.4 1.0 copy-start.17
  75.3 0.8 copy-start.21
  82.0 31.1 %copy-start.8 = (f32[2,256]{1,0:T(2,128)S(1)}, f32[2,256]{1,0:T(2,128)}, u32[]{:S(2)}) copy-start(f32[2,256]{1,0:T(2,128)} %copy-done.7) | copy-start | bytes 6148
  113.2 6.1 %copy-start.24 = (bf16[512,2048]{1,0:T(8,128)(2,1)S(1)}, bf16[512,2048]{1,0:T(8,128)(2,1)}, u32[]{:S(2)}) copy-start(bf16[512,2048]{1,0:T(8,128)(2,1)} %get-tuple-element.17) | copy-start | bytes 6291460
  113.2 6.1 %copy-start.30 = (bf16[2048,512]{1,0:T(8,128)(2,1)S(1)}, bf16[2048,512]{1,0:T(8,128)(2,1)}, u32[]{:S(2)}) copy-start(bf16[2048,512]{1,0:T(8,128)(2,1)} %param.27) | copy-start | bytes 6291460
  119.3 2.1 %copy-start.19 = (f32[2,256,512]{2,1,0:T(8,128)}, f32[2,256,512]{2,1,0:T(8,128)S(1)}, u32[]{:S(2)}) copy-start(f32[2,256,512]{2,1,0:T(8,128)S(1)} %shard_map.174.start_ref) | copy-start | bytes 3145732
  119.3 2.1 %copy-start.6 = (f32[2,256]{1,0:T(2,128)S(1)}, f32[2,256]{1,0:T(2,128)}, u32[]{:S(2)}) copy-start(f32[2,256]{1,0:T(2,128)} %copy-done.5) | copy-start | bytes 6148
  119.3 16.2 %copy-start.15 = (f32[512]{0:T(512)S(1)}, f32[512]{0:T(512)}, u32[]{:S(2)}) copy-start(f32[512]{0:T(512)} %param.32) | copy-start | bytes 6148
  135.5 1.6 copy-start.9
  137.1 1.0 copy-start.16
  138.1 1.2 copy-start.18
  139.3 1.2 copy-start.20
  140.6 1.0 copy-start.22
  143.2 13.3 %copy-start.4 = (f32[1,2048]{1,0:T(1,128)S(1)}, f32[1,2048]{1,0:T(1,128)}, u32[]{:S(2)}) copy-start(f32[1,2048]{1,0:T(1,128)} %copy-done.3) | copy-start | bytes 24580
  156.5 5.1 %copy-start.26 = (f32[2048]{0:T(1024)S(1)}, f32[2048]{0:T(1024)}, u32[]{:S(2)}) copy-start(f32[2048]{0:T(1024)} %param.35) | copy-start | bytes 24580
  156.5 5.1 %copy-start.27 = (f32[2048]{0:T(1024)S(1)}, f32[2048]{0:T(1024)}, u32[]{:S(2)}) copy-start(f32[2048]{0:T(1024)} %param.34) | copy-start | bytes 24580
Sparse Core Ops, SparseCore 0:
  8.9 69.7 all-gather.5
  80.2 55.1 all-gather.7
